TPU v7x, 512 devices: a whole 4x4x16 slice. The times are simulated.
512 devices in a mesh: sp: 64 (over z, y), tp: 8 (over x, core).
Axes of the slice: x: 4, y: 4, z: 16, core: 2. Of those that a mesh axis runs over, the one named last changes fastest.
Arguments:
- acceptor_signal: bfloat16 [8192, 1024], P('sp', 'tp'), may hold values from -6 to 6
- address_entries: bfloat16 [8192, 1024], P('sp', 'tp'), may hold values from -6 to 6
- payload_entries: bfloat16 [8192, 1024], P('sp', 'tp'), may hold values from -6 to 6
- fading_logits: float32 [8192, 1024], P('sp', 'tp'), may hold values from -12 to -2
- learning_rate_logits: float32 [8192, 1024], P('sp', 'tp'), may hold values from -10 to 4
- exit_switch_entries: bfloat16 [8192, 1024], P('sp', 'tp'), may hold values from -6 to 6
- extra_reward_weights: float32 [1024], P('tp'), may hold values from -0.3 to 0.3
- subspace_rescale_weights: float32 [1024], P('tp'), may hold values from 0.1 to 1.9
- timemix_exit_weights: bfloat16 [1024, 2048], P('tp'), may hold values from -0.1875 to 0.1875
- skip_stream_arriving: bfloat16 [8192, 2048], P(('sp', 'tp')), may hold values from -6 to 6
- pointwise_block_scaling: float32 [2048], replicated, may hold values from 0.1 to 1.9
- switch_projection: bfloat16 [2048, 5632], P('sp', 'tp'), may hold values from -0.125 to 0.125
- widening_projection: bfloat16 [2048, 5632], P('sp', 'tp'), may hold values from -0.125 to 0.125
- switch_filter_coefficients: float32 [3, 5632], P(None, 'tp'), may hold values from -3.5 to 3.5
- narrowing_projection: bfloat16 [5632, 2048], P('tp', 'sp'), may hold values from -0.078125 to 0.078125
Outputs:
- layer_out: bfloat16 [8192, 2048], P(('sp', 'tp'))
All inputs are finite; a program needn't handle non-finite values.
Results may differ from a plain program's by a relative error of at most 0.019.
Values may be sent and summed in bfloat16 or wider, within the bound.
A program may use at most 64 MiB of HBM per device.

v0:
```python
import jax
import jax.numpy as jnp
from jax import lax
from jax.sharding import Mesh
from jax.sharding import PartitionSpec as P

SUBSPACE_WIDTH = 64
SPAN = 16
SP = ("sp_0", "sp_1")
SP_TP = ("sp_0", "sp_1", "tp")


group_eps = 0.00064
norm_eps = 1e-06
highest = lax.Precision.HIGHEST


def nothing_yet(shard, identity):
    return jax.tree.map(
        lambda part, zero: jnp.zeros_like(part) + jnp.asarray(zero, part.dtype), shard, identity
    )


def gathered_once(shard, axis):
    leaves = jax.tree.leaves(shard)
    order = sorted(range(len(leaves)), key=lambda k: -leaves[k].size)
    width = (1, *leaves[order[0]].shape)[-1]
    lines = [
        jnp.pad(leaves[k].reshape(-1), (0, -leaves[k].size % width)).reshape(-1, width)
        for k in order
    ]
    both, at, found = (lax.all_gather(jnp.concatenate(lines), axis), 0, {})
    for k, line in zip(order, lines):
        share = both[:, at : at + len(line)].reshape(len(both), -1)
        found[k] = share[:, : leaves[k].size].reshape(-1, *leaves[k].shape)
        at += len(line)
    numbers = iter(range(len(leaves)))
    return jax.tree.map(lambda _: found[next(numbers)], shard)


def entering(shard, axes, combine, identity):
    before = start = nothing_yet(shard, identity)
    subtotal = shard
    for axis in reversed(axes):
        count, position = (lax.axis_size(axis), lax.axis_index(axis))
        pieces = gathered_once(
            jax.tree.map(
                lambda part, kind: part.astype(kind), subtotal, (jnp.bfloat16, jnp.bfloat16)
            ),
            axis,
        )
        inside, subtotal = (start, start)
        for k in range(count):
            passed = k < position
            subtotal = combine(
                subtotal, jax.tree.map(lambda part, own: part[k].astype(own.dtype), pieces, shard)
            )
            inside = jax.tree.map(lambda new, old: jnp.where(passed, new, old), subtotal, inside)
        before = combine(inside, before)
    return before


def turned_gather(arrays, axis, dims):
    turned = [jnp.moveaxis(a, dim, 0) for a, dim in zip(arrays, dims)]
    both = jnp.concatenate([t.reshape(len(t), -1) for t in turned], axis=1)
    whole, at, finished = (lax.all_gather(both, axis, axis=0, tiled=True), 0, [])
    for t, dim in zip(turned, dims):
        share = whole[:, at : at + t[0].size].reshape(-1, *t.shape[1:])
        finished.append(jnp.moveaxis(share, 0, dim))
        at += t[0].size
    return tuple(finished)


def in_blocks(shard, dim, count):
    before, after = (shard.shape[:dim], shard.shape[dim + 1 :])
    return jnp.moveaxis(shard.reshape(*before, count, -1, *after), dim, 0)


def summed_on_arrival(shard, axis, dim):
    count = lax.axis_size(axis)
    tiles = lax.all_to_all(in_blocks(shard, dim, count), axis, 0, 0, tiled=True)
    return jnp.sum(tiles.astype(jnp.float32), axis=0)


def laid_out(tiles, dim):
    tiles = jnp.moveaxis(tiles, 0, dim)
    shape = tiles.shape
    return tiles.reshape(*shape[:dim], shape[dim] * shape[dim + 1], *shape[dim + 2 :])


def from_everyone(shard, axis):
    copies = jnp.broadcast_to(shard, (lax.axis_size(axis), *shard.shape))
    return lax.all_to_all(copies, axis, split_axis=0, concat_axis=0, tiled=True)


def collect(shard, axis, dim):
    return laid_out(from_everyone(shard, axis), dim)


def shifted(block, axis, distance):
    devices = range(lax.axis_size(axis))
    route = [(i - distance, i) for i in devices if i - distance in devices]
    return lax.ppermute(block, axis, route)


def by_heads(array):
    return array.astype(jnp.float32).reshape(array.shape[0], -1, SUBSPACE_WIDTH)


def mechanism_inputs(
    acceptor_signal, address_entries, payload_entries, fading_logits, learning_rate_logits
):
    acceptor_entries = by_heads(acceptor_signal)
    address_mapped = by_heads(address_entries)
    payload_mapped = by_heads(payload_entries)
    log_rate = -jax.nn.softplus(-fading_logits) - 0.5
    fading = by_heads(jnp.exp(-jnp.exp(log_rate)))
    erase_rate = by_heads(jax.nn.sigmoid(learning_rate_logits))
    length = jnp.sqrt(jnp.sum(address_mapped * address_mapped, axis=-1, keepdims=True))
    unit_key = address_mapped / jnp.maximum(length, 1.0)
    return (
        acceptor_entries,
        address_mapped,
        payload_mapped,
        fading,
        -unit_key,
        unit_key * erase_rate,
    )


def subspace_outcomes(
    acceptor_entries,
    address_mapped,
    payload_mapped,
    closing_memory,
    subspace_rescale_weights,
    extra_reward_weights,
    exit_switch_entries,
):
    centred = closing_memory - jnp.mean(closing_memory, axis=-1, keepdims=True)
    rescaled_arguments = centred * lax.rsqrt(
        jnp.mean(centred * centred, axis=-1, keepdims=True) + group_eps
    )
    scaling_fetch = subspace_rescale_weights.reshape(-1, SUBSPACE_WIDTH)
    extra_reward_fetch = extra_reward_weights.reshape(-1, SUBSPACE_WIDTH)
    present_extra_reward = (
        jnp.sum(acceptor_entries * address_mapped * extra_reward_fetch, axis=-1, keepdims=True)
        * payload_mapped
    )
    timemix_product = rescaled_arguments * scaling_fetch + present_extra_reward
    timemix_product = timemix_product.reshape(
        timemix_product.shape[0], -1
    ) * exit_switch_entries.astype(jnp.float32)
    return timemix_product.astype(jnp.bfloat16)


def compose(earlier, latter):
    mapping = jnp.einsum("...ij,...jk->...ik", earlier[0], latter[0], precision=highest)
    state = jnp.einsum("...ij,...jk->...ik", earlier[1], latter[0], precision=highest) + latter[1]
    return (mapping, state)


def span_step(carried, sublevel_arguments):
    state, mapping = carried
    acceptor_entries, address_mapped, payload_mapped, fading, erase_dir, erase_amt = (
        sublevel_arguments
    )
    along = jnp.einsum("bhij,bhj->bhi", state, erase_dir, precision=highest)
    map_along = jnp.einsum("bhij,bhj->bhi", mapping, erase_dir, precision=highest)
    state = (
        state * fading[:, :, None, :]
        + along[..., None] * erase_amt[:, :, None, :]
        + payload_mapped[..., None] * address_mapped[:, :, None, :]
    )
    mapping = mapping * fading[:, :, None, :] + map_along[..., None] * erase_amt[:, :, None, :]
    local_out = jnp.einsum("bhij,bhj->bhi", state, acceptor_entries, precision=highest)
    probe = jnp.einsum("bhij,bhj->bhi", mapping, acceptor_entries, precision=highest)
    return ((state, mapping), (local_out, probe))


def recurrence(sublevel_arguments):
    token_count, head_count = (sublevel_arguments[0].shape[0], sublevel_arguments[0].shape[1])
    blocks = token_count // SPAN

    def arrange(member):
        return jnp.moveaxis(member.reshape(blocks, SPAN, head_count, SUBSPACE_WIDTH), 1, 0)

    arranged = tuple((arrange(member) for member in sublevel_arguments))
    unit_map = jnp.eye(SUBSPACE_WIDTH, dtype=jnp.float32)
    zero_state = jnp.zeros((blocks, head_count, SUBSPACE_WIDTH, SUBSPACE_WIDTH), jnp.float32)
    start_maps = jnp.broadcast_to(unit_map, zero_state.shape)
    (block_states, block_maps), (local_out, probe) = lax.scan(
        span_step, (zero_state, start_maps), arranged
    )
    cum_maps, cum_states = lax.associative_scan(compose, (block_maps, block_states))
    head_unit = jnp.broadcast_to(unit_map, (head_count, SUBSPACE_WIDTH, SUBSPACE_WIDTH))
    head_zero = jnp.zeros((head_count, SUBSPACE_WIDTH, SUBSPACE_WIDTH), jnp.float32)
    _, incoming = entering((cum_maps[-1], cum_states[-1]), SP, compose, (head_unit, head_zero))
    prior_maps = jnp.concatenate([head_unit[None], cum_maps[:-1]], axis=0)
    prior_states = jnp.concatenate([head_zero[None], cum_states[:-1]], axis=0)
    entry = jnp.einsum("hij,bhjk->bhik", incoming, prior_maps, precision=highest) + prior_states
    closing_memory = local_out + jnp.einsum("bhij,tbhj->tbhi", entry, probe, precision=highest)
    return jnp.moveaxis(closing_memory, 0, 1).reshape(token_count, head_count, SUBSPACE_WIDTH)


def body(
    acceptor_signal,
    address_entries,
    payload_entries,
    fading_logits,
    learning_rate_logits,
    exit_switch_entries,
    extra_reward_weights,
    subspace_rescale_weights,
    timemix_exit_weights,
    skip_stream_arriving,
    pointwise_block_scaling,
    switch_projection,
    widening_projection,
    switch_filter_coefficients,
    narrowing_projection,
):
    gate_full, up_full, down_full = turned_gather(
        (switch_projection, widening_projection, narrowing_projection), SP, (0, 0, 1)
    )
    sublevel_arguments = mechanism_inputs(
        acceptor_signal, address_entries, payload_entries, fading_logits, learning_rate_logits
    )
    closing_memory = recurrence(sublevel_arguments)
    timemix_product = subspace_outcomes(
        sublevel_arguments[0],
        sublevel_arguments[1],
        sublevel_arguments[2],
        closing_memory,
        subspace_rescale_weights,
        extra_reward_weights,
        exit_switch_entries,
    )
    token_count = timemix_product.shape[0]
    picked = timemix_product
    attended = summed_on_arrival(
        jnp.dot(picked, timemix_exit_weights, preferred_element_type=jnp.float32).astype(
            jnp.bfloat16
        ),
        "tp",
        0,
    )
    hidden_res = skip_stream_arriving.astype(jnp.float32) + attended
    rescaled_arguments = (
        hidden_res
        * lax.rsqrt(jnp.mean(hidden_res * hidden_res, axis=-1, keepdims=True) + norm_eps)
        * pointwise_block_scaling
    )
    rescaled_arguments = rescaled_arguments.astype(jnp.bfloat16)
    all_rows = collect(rescaled_arguments, "tp", 0)
    gate_acc = jnp.dot(all_rows, gate_full, preferred_element_type=jnp.float32)
    up_acc = jnp.dot(all_rows, up_full, preferred_element_type=jnp.float32)
    gate_pre = gate_acc.astype(jnp.bfloat16)
    up_part = up_acc.astype(jnp.bfloat16)
    taps = switch_filter_coefficients.shape[0]
    tail_rows = shifted(gate_pre[token_count - taps + 1 :], SP, 1)
    extended = jnp.concatenate([tail_rows, gate_pre], axis=0).astype(jnp.float32)
    conv_out = jnp.zeros(gate_pre.shape, jnp.float32)
    for tap in range(taps):
        conv_out = conv_out + switch_filter_coefficients[tap] * extended[tap : tap + token_count]
    hidden = (jax.nn.silu(conv_out) * up_part.astype(jnp.float32)).astype(jnp.bfloat16)
    picked = hidden
    projected = summed_on_arrival(
        jnp.dot(picked, down_full, preferred_element_type=jnp.float32).astype(jnp.bfloat16), "tp", 0
    )
    return (hidden_res + projected).astype(jnp.bfloat16)


def solution(mesh):
    finer = Mesh(mesh.devices.reshape(16, 4, mesh.shape["tp"]), ("sp_0", "sp_1", "tp"))
    placed = (
        P(SP, "tp"),
        P(SP, "tp"),
        P(SP, "tp"),
        P(SP, "tp"),
        P(SP, "tp"),
        P(SP, "tp"),
        P("tp"),
        P("tp"),
        P("tp", None),
        P(SP_TP, None),
        P(),
        P(SP, "tp"),
        P(SP, "tp"),
        P(None, "tp"),
        P("tp", SP),
    )
    return jax.shard_map(
        body, mesh=finer, in_specs=placed, out_specs=P(SP_TP, None), check_vma=False
    )
```

profile of v0, /device:TPU:32, one launch (start us, length us, event | category | flops | bytes accessed | tf_op | source)
XLA Modules:
  0.0 274.5 jit_solution(6896397851667310387)
XLA Ops:
  6.5 1.7 concatenate.38
  14.0 118.5 %while.17 = (s32[]{:T(128)}, f32[8,2,64,64]{3,2,1,0:T(8,128)S(1)}, f32[8,2,64,64]{3,2,1,0:T(8,128)S(1)}, f32[16,8,2,64]{3,0,2,1:T(8,128)}, f32[16,8,2,64]{3,0,2,...) while((s32[]{:T(128)}, f32[8,2,64,64]{3,2,1,0:T(8,128)S(1)}, ...), condition=%wide.region_2.3_spmd.clone, body=%wide.region_1.2_spmd.clone.sunk | while | flops 3801091 | bytes 2220188 | solution.py:192
  17.4 1.5 dynamic_update_slice.12
  19.9 1.5 dynamic_update_slice.11
  24.8 1.5 dynamic_update_slice.12
  27.3 1.5 dynamic_update_slice.11
  32.2 1.5 dynamic_update_slice.12
  34.7 1.5 dynamic_update_slice.11
  39.6 1.5 dynamic_update_slice.12
  42.1 1.5 dynamic_update_slice.11
  54.4 1.5 dynamic_update_slice.12
  61.8 1.5 dynamic_update_slice.12
  69.2 1.5 dynamic_update_slice.12
  76.6 1.5 dynamic_update_slice.12
  84.0 1.5 dynamic_update_slice.12
  91.4 1.5 dynamic_update_slice.12
  98.8 1.5 dynamic_update_slice.12
  106.3 1.5 dynamic_update_slice.12
  113.7 1.5 dynamic_update_slice.12
  121.1 1.5 dynamic_update_slice.12
  128.5 1.5 dynamic_update_slice.12
  130.9 1.5 dynamic_update_slice.11
  137.9 3.3 %pad.120 = f32[7,2,64,64]{3,2,1,0:T(8,128)} pad(f32[4,2,64,64]{3,2,1,0:T(8,128)S(1)} %add.191, f32[]{:T(128)} %constant.21.clone.1), padding=0_0_1x0_0_0x0_0_0x0_0_0 | pad | bytes 360452
  143.6 12.8 %all-gather = bf16[1024,64]{1,0:T(8,128)(2,1)S(1)} all-gather(bf16[256,64]{1,0:T(8,128)(2,1)S(1)} %pad_maximum_fusion.4), channel_id=2, replica_groups=mesh['sp_0'=16,'sp_1'=4,'tp'=8] {'sp_1'}, dimensions={0}, use_global_device_ids=true | all-gather | bytes 163840 | tf_op jit(solution)/shard_map/all_gather | solution.py:32
  157.8 40.8 %all-gather.1 = bf16[4096,64]{1,0:T(8,128)(2,1)S(1)} all-gather(bf16[256,64]{1,0:T(8,128)(2,1)S(1)} %pad_maximum_fusion.5), channel_id=3, replica_groups=mesh['sp_0'=16,'sp_1'=4,'tp'=8] {'sp_0'}, dimensions={0}, use_global_device_ids=true | all-gather | bytes 557056 | tf_op jit(solution)/shard_map/all_gather | solution.py:32
  205.3 14.6 %all_to_all.15 = bf16[8,16,2048]{2,1,0:T(8,128)(2,1)S(1)} all-to-all(bf16[8,16,2048]{2,1,0:T(8,128)(2,1)S(1)} %bitcast.274), channel_id=1, replica_groups=mesh['sp_0'=16,'sp_1'=4,'tp'=8] {'tp'}, dimensions={0} | all-to-all | bytes 1048576 | tf_op jit(solution)/shard_map/all_to_all | solution.py:81
  220.3 12.8 %all_to_all.16 = bf16[8,16,2048]{2,1,0:T(8,128)(2,1)S(1)} all-to-all(bf16[8,16,2048]{2,1,0:T(8,128)(2,1)S(1)} %broadcast_in_dim.46), channel_id=1, replica_groups=mesh['sp_0'=16,'sp_1'=4,'tp'=8] {'tp'}, dimensions={0} | all-to-all | bytes 1048576 | tf_op jit(solution)/shard_map/all_to_all | solution.py:93
  233.0 3.2 %fusion.16 = bf16[128,704]{0,1:T(8,128)(2,1)S(1)} fusion(bf16[128,2048]{1,0:T(8,128)(2,1)S(1)} %bitcast.283, bf16[2048,2112]{1,0:T(8,128)(2,1)} %all-gather.4.cloned.1.call-done), kind=kOutput, calls=%fused_computation.26 | convolution fusion | flops 369188864 | bytes 3850240 | tf_op jit(solution)/shard_map/dot_general | solution.py:256
  236.3 2.4 collective-permute-start
  238.8 7.4 %collective-permute-done = bf16[2,704]{0,1:T(8,128)(2,1)S(1)} collective-permute-done((bf16[2,704]{0,1:T(8,128)(2,1)S(1)}, bf16[2,704]{0,1:T(8,128)(2,1)S(1)}, u32[]{:S(2)}, u32[]{:S(2)}) %collective-permute-start) | collective-permute-done | bytes 2848 | tf_op jit(solution)/shard_map/ppermute | solution.py:103
  246.4 7.8 %fusion.12 = bf16[128,2048]{1,0:T(8,128)(2,1)S(1)} fusion(bf16[2048,2112]{1,0:T(8,128)(2,1)} %all-gather.4.cloned.1.call-done, bf16[128,2048]{1,0:T(8,128)(2,1)S(1)} %bitcast.284, f32[130,704]{0,1:T(8,128)S(1)} %maximum_convert_fusion, f32[704]{0:T(1024)S(1)} %get-tuple-element.139, f32[704]{0:T(1024)S(1)} %get-tuple-element.140, ...), kind=kOutput, calls=%fused_computation.22 | convolution fusion | flops 739631104 | bytes 8433664 | tf_op jit(solution)/shard_map/dot_general | solution.py:269
  254.2 12.8 %all_to_all.17 = bf16[8,16,2048]{2,1,0:T(8,128)(2,1)S(1)} all-to-all(bf16[8,16,2048]{2,1,0:T(8,128)(2,1)S(1)} %bitcast.285), channel_id=1, replica_groups=mesh['sp_0'=16,'sp_1'=4,'tp'=8] {'tp'}, dimensions={0} | all-to-all | bytes 1048576 | tf_op jit(solution)/shard_map/all_to_all | solution.py:81
  (283 shorter events, 110.0 us)
Async XLA Ops:
  6.5 198.4 %copy-start = (bf16[128,2048]{1,0:T(8,128)(2,1)S(1)}, bf16[128,2048]{1,0:T(8,128)(2,1)}, u32[]{:S(2)}) copy-start(bf16[128,2048]{1,0:T(8,128)(2,1)} %param.25) | copy-start | bytes 1572868
  6.5 226.5 %all-gather.4.cloned.1.call-start = ((), (), s32[]{:S(2)}) async-start(), calls=%async_computation.3 | async-start | bytes 9052160 | tf_op jit(solution)/shard_map/all_gather | solution.py:66
  142.5 60.2 %copy-start.2 = (f32[16,8,2,64]{3,0,2,1:T(8,128)S(1)}, f32[16,8,2,64]{3,0,2,1:T(8,128)}, u32[]{:S(2)}) copy-start(f32[16,8,2,64]{3,0,2,1:T(8,128)} %get-tuple-element.65) | copy-start | bytes 196612
  142.5 60.2 %copy-start.3 = (f32[16,8,2,64]{3,0,2,1:T(8,128)S(1)}, f32[16,8,2,64]{3,0,2,1:T(8,128)}, u32[]{:S(2)}) copy-start(f32[16,8,2,64]{3,0,2,1:T(8,128)} %get-tuple-element.66) | copy-start | bytes 196612
  142.5 62.0 %copy-start.9 = (f32[128]{0:T(128)S(1)}, f32[128]{0:T(128)}, u32[]{:S(2)}) copy-start(f32[128]{0:T(128)} %param.23) | copy-start | bytes 1540
  143.5 61.5 %copy-start.4 = (bf16[128,128]{1,0:T(8,128)(2,1)S(1)}, bf16[128,128]{1,0:T(8,128)(2,1)}, u32[]{:S(2)}) copy-start(bf16[128,128]{1,0:T(8,128)(2,1)} %param.19) | copy-start | bytes 98308
  143.5 61.5 %copy-start.5 = (bf16[128,128]{1,0:T(8,128)(2,1)S(1)}, bf16[128,128]{1,0:T(8,128)(2,1)}, u32[]{:S(2)}) copy-start(bf16[128,128]{1,0:T(8,128)(2,1)} %param.22) | copy-start | bytes 98308
  143.5 61.5 %copy-start.8 = (f32[128]{0:T(128)S(1)}, f32[128]{0:T(128)}, u32[]{:S(2)}) copy-start(f32[128]{0:T(128)} %param.24) | copy-start | bytes 1540
  157.7 62.2 %copy-start.1 = (bf16[16,2048]{1,0:T(8,128)(2,1)S(1)}, bf16[16,2048]{1,0:T(8,128)(2,1)}, u32[]{:S(2)}) copy-start(bf16[16,2048]{1,0:T(8,128)(2,1)} %param.26) | copy-start | bytes 196612
  198.5 21.6 %copy-start.6 = (f32[2048]{0:T(1024)S(1)}, f32[2048]{0:T(1024)}, u32[]{:S(2)}) copy-start(f32[2048]{0:T(1024)} %param.27) | copy-start | bytes 24580
  201.5 37.3 %copy-start.7 = (f32[3,704]{1,0:T(4,128)S(1)}, f32[3,704]{1,0:T(4,128)}, u32[]{:S(2)}) copy-start(f32[3,704]{1,0:T(4,128)} %param.30) | copy-start | bytes 25348
  236.3 9.9 %collective-permute-start = (bf16[2,704]{0,1:T(8,128)(2,1)S(1)}, bf16[2,704]{0,1:T(8,128)(2,1)S(1)}, u32[]{:S(2)}, u32[]{:S(2)}) collective-permute-start(bf16[2,704]{0,1:T(8,128)(2,1)S(1)} %slice.463), channel_id=1, source_target_pairs={{0,8},{8,16},{16,24},{24,32},{32,40},{40,48},{48,56},{56,64},{64,7... | collective-permute-start | bytes 8456 | tf_op jit(solution)/shard_map/ppermute | solution.py:103
Sparse Core Ops, SparseCore 0:
  10.3 161.9 all-gather.3
where the time goes:
time: 277 us; the launch traced here: 275 us
  blocking collectives  93.6 us (34%)
  matrix products  79.1 us (29%)
  local copies, waits for them, and re-layouts  60.8 us (22%)
  other arithmetic  16.3 us (6%)
  between operations  14.4 us (5%)
  waiting for transfers between devices  7.45 us (3%)
    all_gather x2, blocking collectives, gathered_once(): both, at, found = (lax.all_gather(jnp.concatenate(lines), axis), 0, {})  53.5 us
    dynamic_update_slice x32, local copies, waits for them, and re-layouts, recurrence(): lax.scan(span_step, (zero_state, start_maps), arranged)  48.4 us
    all_to_all x2, blocking collectives, summed_on_arrival(): tiles = lax.all_to_all(in_blocks(shard, dim, count), axis, 0, 0, tiled=True)  27.3 us
    dot_general x16, matrix products, span_step(): jnp.einsum('bhij,bhj->bhi', mapping, erase_dir, precision=highest)  14.8 us
    dot_general x16, matrix products, span_step(): along = jnp.einsum('bhij,bhj->bhi', state, erase_dir, precision=highest)  14.8 us
    dot_general x16, matrix products, span_step(): jnp.einsum('bhij,bhj->bhi', mapping, acceptor_entries, precision=highest)  14.7 us
    dot_general x16, matrix products, span_step(): jnp.einsum('bhij,bhj->bhi', state, acceptor_entries, precision=highest)  14.7 us
    all_to_all x1, blocking collectives, from_everyone(): return lax.all_to_all(copies, axis, split_axis=0, concat_axis=0, tiled=True)  12.8 us
  transfers between devices with their start and end apart: 2, of which 1 were waited for; matrix products, arithmetic and copies ran while one was open for 52% of the time, Pallas kernels for 0%

commit v1 on v0

v1 whole, which is shorter than its diff:
```python
import functools

import jax
import jax.numpy as jnp
from jax import lax
from jax.experimental import pallas as pl
from jax.experimental.pallas import tpu as pltpu
from jax.sharding import Mesh
from jax.sharding import PartitionSpec as P

WIDTH = 64
SP = ("sp_0", "sp_1")
SP_TP = ("sp_0", "sp_1", "tp")
COLUMNS = 4
MESH = pl.DeviceIdType.MESH

group_eps = 0.00064
norm_eps = 1e-06
f32 = jnp.float32
bf16 = jnp.bfloat16

NN = (((1,), (0,)), ((), ()))
NT = (((1,), (1,)), ((), ()))
TN = (((0,), (0,)), ((), ()))


def exact(a, b, dims=NN):
    return lax.dot_general(
        a, b, dims, precision=lax.Precision.HIGHEST, preferred_element_type=f32
    )


def plain(a, b, dims=NN):
    return lax.dot_general(a, b, dims, preferred_element_type=f32)


def iota(shape, dim):
    return lax.broadcasted_iota(jnp.int32, shape, dim)


def ring_index(base, step, size):
    return lax.rem(base + step + size, size)


def head_blocks(n):
    return (iota((n, n), 0) // WIDTH) == (iota((n, n), 1) // WIDTH)


def packed(mapping, state):
    return jnp.concatenate(
        [mapping[:WIDTH] + mapping[WIDTH:], state[:WIDTH] + state[WIDTH:]], axis=0
    ).astype(bf16)


def unpacked(block):
    block = block.astype(f32)
    same = head_blocks(2 * WIDTH)
    mapping, state = block[:WIDTH], block[WIDTH:]
    mapping = jnp.where(same, jnp.concatenate([mapping, mapping], axis=0), 0.0)
    state = jnp.where(same, jnp.concatenate([state, state], axis=0), 0.0)
    return mapping, state


def compose(earlier, latter):
    both = exact(latter[0], jnp.concatenate(earlier, axis=1))
    n = 2 * WIDTH
    return both[:, :n], both[:, n:] + latter[1]


def folded(slots, count, position):
    n = 2 * WIDTH
    eye = jnp.where(iota((n, n), 0) == iota((n, n), 1), 1.0, 0.0)
    before = (eye, jnp.zeros((n, n), f32))
    total = unpacked(slots[0])
    for k in range(1, count):
        hit = position == k
        before = tuple(jnp.where(hit, new, old) for new, old in zip(total, before))
        total = compose(total, unpacked(slots[k]))
    return before, total


def block_inverse(strict):
    n = strict.shape[0]
    row, col = iota((n, n), 0), iota((n, n), 1)
    found = jnp.where(row == col, 1.0, 0.0) + jnp.where(row // 2 == col // 2, strict, 0.0)
    m = 2
    while m < n:
        edge = jnp.where((row // (2 * m) == col // (2 * m)) & (row // m != col // m), strict, 0.0)
        found = found + exact(found, exact(edge, found))
        m *= 2
    return found


def local_mixer(r_ref, k_ref, v_ref, fade_ref, rate_ref):
    r, k, v = r_ref[...].astype(f32), k_ref[...].astype(f32), v_ref[...].astype(f32)
    n = r.shape[0]
    row, col = iota((n, n), 0), iota((n, n), 1)
    ones = jnp.where(head_blocks(n), 1.0, 0.0)
    log_fade = -jax.nn.sigmoid(fade_ref[...]) * 0.6065306597126334
    total_log = exact(jnp.where(row >= col, 1.0, 0.0), log_fade)
    length = jnp.sqrt(exact(k * k, ones))
    unit = k / jnp.maximum(length, 1.0)
    amount = unit * jax.nn.sigmoid(rate_ref[...])
    kept = jnp.exp(total_log)
    grown = jnp.exp(-total_log)
    erase = -unit * jnp.exp(total_log - log_fade)
    read = r * kept
    amount_grown, key_grown = amount * grown, k * grown
    last = kept[n - 1 :, :]
    right = jnp.concatenate([amount_grown, key_grown], axis=0)
    strict, lower = row > col, row >= col
    maps = jnp.zeros((n, n), f32)
    values = jnp.zeros((n, n), f32)
    probe, local_out = read, jnp.zeros((n, n), f32)
    for h in range(n // WIDTH):
        mine = col // WIDTH == h
        erase_h = jnp.where(mine, erase, 0.0)
        read_h = jnp.where(mine, read, 0.0)
        value_h = jnp.where(mine, v, 0.0)
        grams = exact(jnp.concatenate([erase_h, read_h], axis=0), right, NT)
        inverse = block_inverse(jnp.where(strict, grams[:n, :n], 0.0))
        pushed = exact(jnp.where(strict, grams[:n, n:], 0.0), value_h)
        solved = exact(inverse, jnp.concatenate([erase_h, pushed], axis=1))
        shown = exact(jnp.where(lower, grams[n:, :n], 0.0), solved)
        local_out = local_out + shown[:, n:]
        local_out = local_out + exact(jnp.where(lower, grams[n:, n:], 0.0), value_h)
        probe = probe + shown[:, :n]
        maps = maps + solved[:, :n]
        values = values + solved[:, n:]
    same = head_blocks(n)
    amount_end, key_end = amount_grown * last, key_grown * last
    mapping = jnp.where(row == col, last, 0.0) + jnp.where(same, exact(amount_end, maps, TN), 0.0)
    state = jnp.where(same, exact(amount_end, values, TN) + exact(key_end, v, TN), 0.0)
    return mapping, state, probe, local_out


def mixer_kernel(
    nz, ny, span, r_ref, k_ref, v_ref, fade_ref, rate_ref, switch_ref, bonus_ref, rescale_ref,
    gate_ref, up_ref, down_ref, mixed_ref, full_ref,
    near, mid, far, pieces, parts, probe_ref, local_ref, before_ref, carry_ref,
    near_send, near_recv, mid_send, mid_recv, far_send, far_recv, part_send, part_recv,
    plus_send, plus_recv, minus_send, minus_recv,
):
    z, y = lax.axis_index("sp_0"), lax.axis_index("sp_1")
    groups = nz // span
    inner, outer = lax.rem(z, span), z // span
    n = 2 * WIDTH
    units = full_ref.shape[1]
    rows = gate_ref.shape[0]

    def along_y(j):
        return {"sp_1": ring_index(y, j, ny)}

    def along_z(to):
        return {"sp_0": to}

    barrier = pltpu.get_barrier_semaphore()
    for j in range(1, ny):
        pl.semaphore_signal(barrier, inc=1, device_id=along_y(j), device_id_type=MESH)
    for j in range(1, nz):
        pl.semaphore_signal(
            barrier, inc=1, device_id=along_z(ring_index(z, j, nz)), device_id_type=MESH
        )

    mapping, state, probe, local_out = local_mixer(r_ref, k_ref, v_ref, fade_ref, rate_ref)
    near[y] = packed(mapping, state)
    probe_ref[...] = probe
    local_ref[...] = local_out

    eye = jnp.where(iota((rows, rows), 0) == iota((rows, rows), 1), 1.0, 0.0).astype(bf16)
    down_turned = plain(eye, down_ref[...], NT).astype(bf16)
    stacked = jnp.concatenate([gate_ref[...], up_ref[...], down_turned], axis=0)
    wide = pieces.shape[2]
    tall = stacked.shape[1]
    for part in range(ny):
        at, to = iota((tall, wide), 0), iota((tall, wide), 1)
        pick = jnp.where((at == to + part * units) & (to < units), 1.0, 0.0).astype(bf16)
        pieces[part] = plain(stacked, pick).astype(bf16)

    pl.semaphore_wait(barrier, ny - 1 + nz - 1)

    def near_copy(source, target):
        return pltpu.make_async_remote_copy(
            src_ref=near.at[source], dst_ref=near.at[source],
            send_sem=near_send.at[target], recv_sem=near_recv.at[target],
            device_id=along_y(target), device_id_type=MESH,
        )

    def part_copy(j, arriving):
        to = ring_index(y, j, ny)
        source = ring_index(y, -j, ny) if arriving else y
        return pltpu.make_async_remote_copy(
            src_ref=pieces.at[to], dst_ref=parts.at[source],
            send_sem=part_send.at[j], recv_sem=part_recv.at[j],
            device_id=along_y(j), device_id_type=MESH,
        )

    for j in range(1, ny):
        near_copy(y, j).start()
    for j in range(1, ny):
        part_copy(j, False).start()
    parts[y] = pieces[y]

    for j in range(1, ny):
        near_copy(ring_index(y, -j, ny), j).wait_recv()
    before, total = folded(near, ny, y)
    before_ref[0] = before[0]
    before_ref[1] = before[1]

    def mid_copy(source, j):
        to = z - inner + ring_index(inner, j, span)
        return pltpu.make_async_remote_copy(
            src_ref=mid.at[source], dst_ref=mid.at[source],
            send_sem=mid_send.at[j], recv_sem=mid_recv.at[j],
            device_id=along_z(to), device_id_type=MESH,
        )

    mid[inner] = packed(*total)
    for j in range(1, span):
        mid_copy(inner, j).start()

    for j in range(1, ny):
        part_copy(j, True).wait_recv()
    square = jnp.where(iota((units, wide), 0) == iota((units, wide), 1), 1.0, 0.0).astype(bf16)
    for c in range(3):
        tallest = jnp.concatenate(
            [parts[part, c * rows : (c + 1) * rows, :] for part in range(ny)], axis=0
        )
        block = plain(square, tallest, NT).astype(bf16)
        full_ref[c, :, pl.ds(pl.multiple_of(z * ny * rows, ny * rows), ny * rows)] = block

    def piece(c, at):
        return full_ref.at[c, :, pl.ds(pl.multiple_of(at * ny * rows, ny * rows), ny * rows)]

    def plus_copy(c, s, at):
        return pltpu.make_async_remote_copy(
            src_ref=piece(c, at), dst_ref=piece(c, at),
            send_sem=plus_send.at[c, s], recv_sem=plus_recv.at[c, s],
            device_id=along_z(ring_index(z, 1, nz)), device_id_type=MESH,
        )

    def minus_copy(c, s, at):
        return pltpu.make_async_remote_copy(
            src_ref=piece(c, at), dst_ref=piece(c, at),
            send_sem=minus_send.at[c, s], recv_sem=minus_recv.at[c, s],
            device_id=along_z(ring_index(z, -1, nz)), device_id_type=MESH,
        )

    n_plus = nz // 2
    n_minus = nz - 1 - n_plus

    def ring_step(s):
        for c in range(3):
            if s > 0 and s <= n_plus:
                plus_copy(c, s - 1, ring_index(z, -s, nz)).wait_recv()
            if s < n_plus:
                plus_copy(c, s, ring_index(z, -s, nz)).start()
            if s > 0 and s <= n_minus:
                minus_copy(c, s - 1, ring_index(z, s, nz)).wait_recv()
            if s < n_minus:
                minus_copy(c, s, ring_index(z, s, nz)).start()

    ring_step(0)

    for j in range(1, span):
        mid_copy(ring_index(inner, -j, span), j).wait_recv()
    before_z, total_z = folded(mid, span, inner)
    before_ref[2] = before_z[0]
    before_ref[3] = before_z[1]

    def far_copy(slot, d, to):
        return pltpu.make_async_remote_copy(
            src_ref=far.at[slot], dst_ref=far.at[slot],
            send_sem=far_send.at[d], recv_sem=far_recv.at[d],
            device_id=along_z(to), device_id_type=MESH,
        )

    far[outer] = packed(*total_z)
    for d in range(1, groups):
        @pl.when(outer + d < groups)
        def _():
            far_copy(outer, d, lax.rem(z + d * span, nz)).start()

    steps = n_plus + 1
    early = min(2, steps - 1)
    for s in range(1, 1 + early):
        ring_step(s)

    carry_ref[...] = jnp.zeros((n, n), f32)
    for g in range(groups - 1):
        @pl.when(outer > g)
        def _():
            for d in range(1, groups):
                @pl.when(outer - g == d)
                def _():
                    far_copy(g, d, lax.rem(z + d * span, nz)).wait_recv()
            step = unpacked(far[g])
            carry_ref[...] = exact(step[0], carry_ref[...]) + step[1]
    incoming = exact(before_ref[2], carry_ref[...]) + before_ref[3]
    incoming = exact(before_ref[0], incoming) + before_ref[1]

    closing = local_ref[...] + exact(probe_ref[...], incoming)
    ones = jnp.where(head_blocks(n), 1.0, 0.0)
    centred = closing - exact(closing, ones) * (1.0 / WIDTH)
    spread = exact(centred * centred, ones) * (1.0 / WIDTH)
    rescaled = centred * lax.rsqrt(spread + group_eps) * rescale_ref[...]
    value = v_ref[...].astype(f32)
    bonus = exact(r_ref[...].astype(f32) * k_ref[...].astype(f32) * bonus_ref[...], ones) * value
    mixed_ref[...] = ((rescaled + bonus) * switch_ref[...].astype(f32)).astype(bf16)

    for s in range(1 + early, steps):
        ring_step(s)

    for j in range(1, ny):
        near_copy(y, j).wait_send()
        part_copy(j, False).wait_send()
    for j in range(1, span):
        mid_copy(inner, j).wait_send()
    for d in range(1, groups):
        @pl.when(outer + d < groups)
        def _():
            far_copy(outer, d, lax.rem(z + d * span, nz)).wait_send()
    for c in range(3):
        for s in range(n_plus):
            plus_copy(c, s, ring_index(z, -s, nz)).wait_send()
        for s in range(n_minus):
            minus_copy(c, s, ring_index(z, s, nz)).wait_send()


def mixer_and_weights(r, k, v, fade, rate, switch, bonus, rescale, gate, up, down):
    nz, ny = lax.axis_size("sp_0"), lax.axis_size("sp_1")
    span = min(4, nz)
    groups = nz // span
    n = r.shape[0]
    rows, hidden = gate.shape
    units = hidden // ny
    wide = -(-units // 128) * 128
    dma = pltpu.SemaphoreType.DMA
    block = pltpu.VMEM((n, n), bf16)
    in_vmem = pl.BlockSpec(memory_space=pltpu.VMEM)
    n_plus = nz // 2
    return pl.pallas_call(
        functools.partial(mixer_kernel, nz, ny, span),
        out_shape=(
            jax.ShapeDtypeStruct((n, n), bf16),
            jax.ShapeDtypeStruct((3, units, nz * ny * rows), bf16),
        ),
        in_specs=[in_vmem] * 11,
        out_specs=(in_vmem, in_vmem),
        scratch_shapes=[
            pltpu.VMEM((ny, n, n), bf16),
            pltpu.VMEM((span, n, n), bf16),
            pltpu.VMEM((groups, n, n), bf16),
            pltpu.VMEM((ny, 3 * rows, wide), bf16),
            pltpu.VMEM((ny, 3 * rows, wide), bf16),
            pltpu.VMEM((n, n), f32),
            pltpu.VMEM((n, n), f32),
            pltpu.VMEM((4, n, n), f32),
            pltpu.VMEM((n, n), f32),
            dma((ny,)), dma((ny,)), dma((span,)), dma((span,)), dma((groups,)), dma((groups,)),
            dma((ny,)), dma((ny,)),
            dma((3, n_plus)), dma((3, n_plus)), dma((3, n_plus)), dma((3, n_plus)),
        ],
        compiler_params=pltpu.CompilerParams(collective_id=0, has_side_effects=True),
        cost_estimate=pl.CostEstimate(flops=2 * 10**9, bytes_accessed=4 * 10**6, transcendentals=0),
        name="mixer",
    )(r, k, v, fade, rate, switch, bonus, rescale, gate, up, down)


def in_blocks(shard, count):
    return shard.reshape(count, -1, shard.shape[1])


def summed_on_arrival(shard, axis):
    count = lax.axis_size(axis)
    tiles = lax.all_to_all(in_blocks(shard, count), axis, 0, 0, tiled=True)
    return jnp.sum(tiles.astype(f32), axis=0)


def body(
    r, k, v, fade, rate, switch, bonus, rescale, exit_weights, skip, scaling, gate, up, taps, down
):
    nz = lax.axis_size("sp_0")
    mixed, weights = mixer_and_weights(
        r, k, v, fade, rate, switch, bonus[None], rescale[None], gate, up, down
    )
    attended = summed_on_arrival(
        jnp.dot(mixed, exit_weights, preferred_element_type=f32).astype(bf16), "tp"
    )
    hidden_res = skip.astype(f32) + attended
    normed = (
        hidden_res
        * lax.rsqrt(jnp.mean(hidden_res * hidden_res, axis=-1, keepdims=True) + norm_eps)
        * scaling
    ).astype(bf16)
    rows = lax.all_gather(normed, ("sp_1", "tp"), tiled=True)
    gate_pre = plain(rows, weights[0], NT).astype(bf16)
    up_part = plain(rows, weights[1], NT).astype(bf16)
    count = taps.shape[0]
    units = gate_pre.shape[1]
    route = [(i, i + 1) for i in range(nz - 1)]
    tail = lax.ppermute(gate_pre[gate_pre.shape[0] - count + 1 :], "sp_0", route)
    mine = lax.dynamic_slice_in_dim(taps, lax.axis_index("sp_1") * units, units, axis=1)
    extended = jnp.concatenate([tail, gate_pre], axis=0).astype(f32)
    conv = jnp.zeros(gate_pre.shape, f32)
    for tap in range(count):
        conv = conv + mine[tap] * extended[tap : tap + gate_pre.shape[0]]
    hidden = (jax.nn.silu(conv) * up_part.astype(f32)).astype(bf16)
    projected = summed_on_arrival(plain(hidden, weights[2]).astype(bf16), ("sp_1", "tp"))
    return (hidden_res + projected).astype(bf16)


def solution(mesh):
    sp, tp = mesh.shape["sp"], mesh.shape["tp"]
    ny = COLUMNS
    finer = Mesh(mesh.devices.reshape(sp // ny, ny, tp), SP_TP)
    cut = P(SP, "tp")
    placed = (
        cut, cut, cut, cut, cut, cut, P("tp"), P("tp"), P("tp", None), P(SP_TP, None), P(),
        cut, cut, P(None, "tp"), P("tp", SP),
    )
    return jax.shard_map(
        body, mesh=finer, in_specs=placed, out_specs=P(SP_TP, None), check_vma=False
    )
```

time: 277 us -> 193 us (0.70)
  the two profiles are of different devices: /device:TPU:32 before, /device:TPU:1 now
where the time goes in v1:
time: 193 us
  Pallas kernels  58.6 us (30%)
  blocking collectives  55.1 us (29%)
  waiting for transfers between devices  50.5 us (26%)
  between operations  13.5 us (7%)
  matrix products  7.27 us (4%)
  starting transfers between devices  3.18 us (2%)
  local copies, waits for them, and re-layouts  2.65 us (1%)
  other arithmetic  2.03 us (1%)
    pallas_call x1, Pallas kernels, mixer_and_weights(): pl.pallas_call(functools.partial(mixer_kernel, nz, ny, span), out_shape=(...  58.6 us
    all_to_all x2, blocking collectives, summed_on_arrival(): tiles = lax.all_to_all(in_blocks(shard, count), axis, 0, 0, tiled=True)  55.1 us
    all_gather x1, waiting for transfers between devices, body(): rows = lax.all_gather(normed, ('sp_1', 'tp'), tiled=True)  50.2 us
    dot_general x2, matrix products, plain(): return lax.dot_general(a, b, dims, preferred_element_type=f32)  6.22 us
  transfers between devices with their start and end apart: 2, of which 2 were waited for; matrix products, arithmetic and copies ran while one was open for 0% of the time, Pallas kernels for 0%

profile of v1, /device:TPU:1, one launch (start us, length us, event | category | flops | bytes accessed | tf_op | source)
XLA Modules:
  0.0 192.8 jit_solution(11583127991579949056)
XLA Ops:
  6.5 0.0 copy-start
  6.5 0.0 all-gather.2.cloned.1.call-start
  6.5 1.7 copy.16.down_ref
  8.2 58.6 %mixer.1 = (bf16[128,128]{1,0:T(8,128)(2,1)}, bf16[3,176,2048]{2,1,0:T(8,128)(2,1)}) custom-call(bf16[128,128]{1,0:T(8,128)(2,1)} %r_ref.1, bf16[128,128]{1,0:T(8,128)(2,1)} %k_ref.1, bf16[128,128]{1,0:T(8,128)(2,1)} %v_ref.1, f32[128,128]{1,0:T(8,128)} %fade_ref.1, f32[128,128]{1,0:T(8,128)} %rate_ref.1, bf16[128,128]{1,0:T(8,128)(2,1)} %switch_ref.1, ...), custom_call_target="tpu_custom_call" | custom-call | flops 2000000000 | bytes 4000000 | tf_op jit(solution)/shard_map/mixer/pallas_call | solution.py:342
  66.8 0.0 copy-start.1
  66.9 0.0 copy-start.2
  66.9 0.0 copy-done
  66.9 1.1 convolution_convert_fusion.1
  67.9 21.0 %all_to_all.10 = bf16[8,16,2048]{2,1,0:T(8,128)(2,1)S(1)} all-to-all(bf16[8,16,2048]{2,1,0:T(8,128)(2,1)S(1)} %bitcast.22), channel_id=1, replica_groups=mesh['sp_0'=16,'sp_1'=4,'tp'=8] {'tp'}, dimensions={0} | all-to-all | bytes 1048576 | tf_op jit(solution)/shard_map/all_to_all | solution.py:376
  88.9 0.1 convert_reduce_fusion.1
  89.0 0.0 copy-done.1
  89.0 0.1 multiply_reduce_fusion
  89.1 0.0 copy-done.2
  89.1 0.7 multiply_convert_fusion
  89.8 0.0 all-gather.2.cloned.1.call-update
  89.9 50.2 %all-gather.2.cloned.1.call-done = bf16[512,2048]{1,0:T(8,128)(2,1)} async-done(((bf16[16,2048]{1,0:T(8,128)(2,1)}), bf16[512,2048]{1,0:T(8,128)(2,1)}) %all-gather.2.cloned.1.call-update) | async-done | bytes 2097168 | tf_op jit(solution)/shard_map/all_gather | solution.py:396
  140.1 2.6 %convolution_convert_fusion.3 = bf16[512,176]{0,1:T(8,128)(2,1)S(1)} fusion(bf16[512,2048]{1,0:T(8,128)(2,1)} %all-gather.2.cloned.1.call-done, bf16[3,176,2048]{2,1,0:T(8,128)(2,1)} %get-tuple-element.8), kind=kOutput, calls=%fused_computation.6 | convolution fusion | flops 369188864 | bytes 2998272 | tf_op jit(solution)/shard_map/dot_general | solution.py:34
  142.7 0.1 slice.40
  142.8 3.2 %collective-permute-start = (bf16[2,176]{0,1:T(8,128)(2,1)S(1)}, bf16[2,176]{0,1:T(8,128)(2,1)S(1)}, u32[]{:S(2)}, u32[]{:S(2)}) collective-permute-start(bf16[2,176]{0,1:T(8,128)(2,1)S(1)} %slice.40), channel_id=1, source_target_pairs={{0,32},{32,64},{64,96},{96,128},{128,160},{160,192},{192,224},{224... | collective-permute-start | bytes 2120 | tf_op jit(solution)/shard_map/ppermute | solution.py:402
  146.0 0.9 constant_dynamic-slice_fusion
  146.8 0.2 collective-permute-done
  147.1 0.1 maximum_convert_fusion
  147.2 3.6 %convolution_convert_fusion = bf16[512,2048]{1,0:T(8,128)(2,1)S(1)} fusion(bf16[512,2048]{1,0:T(8,128)(2,1)} %all-gather.2.cloned.1.call-done, bf16[3,176,2048]{2,1,0:T(8,128)(2,1)} %get-tuple-element.8, f32[514,176]{0,1:T(8,128)S(1)} %maximum_convert_fusion, f32[176]{0:T(256)S(1)} %bitcast.25, f32[176]{0:T(256)S(1)} %bitcast.24, f32[176]{0:T(256)S(1)} %bitcast.23), kind=kOutput, calls=%fused_computation.1 | convolution fusion | flops 740417536 | bytes 6720512 | tf_op jit(solution)/shard_map/dot_general | solution.py:34
  150.8 34.2 %all_to_all.11 = bf16[32,16,2048]{2,1,0:T(8,128)(2,1)S(1)} all-to-all(bf16[32,16,2048]{2,1,0:T(8,128)(2,1)S(1)} %bitcast.21), channel_id=1, replica_groups=mesh['sp_0'=16,'sp_1'=4,'tp'=8] {'sp_1','tp'}, dimensions={0} | all-to-all | bytes 4194304 | tf_op jit(solution)/shard_map/all_to_all | solution.py:376
  185.0 0.3 convert_reduce_fusion
  185.4 0.7 add_convert_fusion
  (1 shorter events, 0.0 us)
Async XLA Ops:
  6.5 60.3 %copy-start = (bf16[128,2048]{1,0:T(8,128)(2,1)S(1)}, bf16[128,2048]{1,0:T(8,128)(2,1)}, u32[]{:S(2)}) copy-start(bf16[128,2048]{1,0:T(8,128)(2,1)} %param.23) | copy-start | bytes 1572868
  6.5 133.5 %all-gather.2.cloned.1.call-start = ((), (), s32[]{:S(2)}) async-start(), calls=%async_computation.2 | async-start | bytes 2162688 | tf_op jit(solution)/shard_map/all_gather | solution.py:396
  66.8 22.1 %copy-start.1 = (bf16[16,2048]{1,0:T(8,128)(2,1)S(1)}, bf16[16,2048]{1,0:T(8,128)(2,1)}, u32[]{:S(2)}) copy-start(bf16[16,2048]{1,0:T(8,128)(2,1)} %param.24) | copy-start | bytes 196612
  66.9 22.3 %copy-start.2 = (f32[2048]{0:T(1024)S(1)}, f32[2048]{0:T(1024)}, u32[]{:S(2)}) copy-start(f32[2048]{0:T(1024)} %param.25) | copy-start | bytes 24580
  142.8 4.3 %collective-permute-start = (bf16[2,176]{0,1:T(8,128)(2,1)S(1)}, bf16[2,176]{0,1:T(8,128)(2,1)S(1)}, u32[]{:S(2)}, u32[]{:S(2)}) collective-permute-start(bf16[2,176]{0,1:T(8,128)(2,1)S(1)} %slice.40), channel_id=1, source_target_pairs={{0,32},{32,64},{64,96},{96,128},{128,160},{160,192},{192,224},{224... | collective-permute-start | bytes 2120 | tf_op jit(solution)/shard_map/ppermute | solution.py:402
Sparse Core Ops, SparseCore 0:
  90.0 50.0 all-gather.1

commit v2 on v1

--- a/solution.py
+++ b/solution.py
@@ -134,14 +134,20 @@
     return mapping, state, probe, local_out
 
 
-def mixer_kernel(
-    nz, ny, span, r_ref, k_ref, v_ref, fade_ref, rate_ref, switch_ref, bonus_ref, rescale_ref,
-    gate_ref, up_ref, down_ref, mixed_ref, full_ref,
-    near, mid, far, pieces, parts, probe_ref, local_ref, before_ref, carry_ref,
+def layer_kernel(
+    nz, ny, nt, span, r_ref, k_ref, v_ref, fade_ref, rate_ref, switch_ref, bonus_ref, rescale_ref,
+    exit_ref, skip_ref, scaling_ref, gate_ref, up_ref, taps_ref, down_ref, out_ref,
+    full_ref, near, mid, far, pieces, parts, probe_ref, local_ref, before_ref, carry_ref,
+    sent, landed, stream_ref, rows_ref, gate_scr, edge_out, edge_in, partial, swapped, summed,
+    first, second, final,
     near_send, near_recv, mid_send, mid_recv, far_send, far_recv, part_send, part_recv,
     plus_send, plus_recv, minus_send, minus_recv,
+    exit_send, exit_recv, one_send, one_recv, two_send, two_recv, pair_send, pair_recv,
+    edge_send, edge_recv, swap_send, swap_recv, first_send, first_recv, last_send, last_recv,
 ):
-    z, y = lax.axis_index("sp_0"), lax.axis_index("sp_1")
+    z, y, t = lax.axis_index("sp_0"), lax.axis_index("sp_1"), lax.axis_index("tp")
+    nx = nt // 2
+    x, core = t // 2, lax.rem(t, 2)
     groups = nz // span
     inner, outer = lax.rem(z, span), z // span
     n = 2 * WIDTH
@@ -160,6 +166,10 @@
     for j in range(1, nz):
         pl.semaphore_signal(
             barrier, inc=1, device_id=along_z(ring_index(z, j, nz)), device_id_type=MESH
+        )
+    for j in range(1, nt):
+        pl.semaphore_signal(
+            barrier, inc=1, device_id={"tp": ring_index(t, j, nt)}, device_id_type=MESH
         )
 
     mapping, state, probe, local_out = local_mixer(r_ref, k_ref, v_ref, fade_ref, rate_ref)
@@ -177,7 +187,7 @@
         pick = jnp.where((at == to + part * units) & (to < units), 1.0, 0.0).astype(bf16)
         pieces[part] = plain(stacked, pick).astype(bf16)
 
-    pl.semaphore_wait(barrier, ny - 1 + nz - 1)
+    pl.semaphore_wait(barrier, ny - 1 + nz - 1 + nt - 1)
 
     def near_copy(source, target):
         return pltpu.make_async_remote_copy(
@@ -282,7 +292,7 @@
             far_copy(outer, d, lax.rem(z + d * span, nz)).start()
 
     steps = n_plus + 1
-    early = min(2, steps - 1)
+    early = min(3, steps - 1)
     for s in range(1, 1 + early):
         ring_step(s)
 
@@ -306,10 +316,191 @@
     rescaled = centred * lax.rsqrt(spread + group_eps) * rescale_ref[...]
     value = v_ref[...].astype(f32)
     bonus = exact(r_ref[...].astype(f32) * k_ref[...].astype(f32) * bonus_ref[...], ones) * value
-    mixed_ref[...] = ((rescaled + bonus) * switch_ref[...].astype(f32)).astype(bf16)
-
-    for s in range(1 + early, steps):
-        ring_step(s)
+    mixed = ((rescaled + bonus) * switch_ref[...].astype(f32)).astype(bf16)
+
+    pending = list(range(1 + early, steps))
+
+    def ring_steps(count):
+        for s in pending[:count]:
+            ring_step(s)
+        del pending[:count]
+
+    own = n // nt
+    width = exit_ref.shape[1]
+
+    def exit_copy(j):
+        to = ring_index(t, j, nt)
+        return pltpu.make_async_remote_copy(
+            src_ref=sent.at[to], dst_ref=landed.at[j],
+            send_sem=exit_send.at[j], recv_sem=exit_recv.at[j],
+            device_id={"tp": to}, device_id_type=MESH,
+        )
+
+    sent[...] = plain(mixed, exit_ref[...]).astype(bf16).reshape(nt, own, width)
+    for j in range(1, nt):
+        exit_copy(j).start()
+    ring_steps(2)
+    attended = sent[t].astype(f32)
+    for j in range(1, nt):
+        exit_copy(j).wait_recv()
+    for j in range(1, nt):
+        attended = attended + landed[j].astype(f32)
+    stream = skip_ref[...].astype(f32) + attended
+    stream_ref[...] = stream
+    mean = jnp.mean(stream * stream, axis=-1, keepdims=True)
+    rows_ref[y, x, core] = (stream * lax.rsqrt(mean + norm_eps) * scaling_ref[...]).astype(bf16)
+
+    across = 1 - core
+    na = ny
+    a, b = y * across + x * core, x * across + y * core
+
+    def place(a_to, b_to):
+        return a_to * across + b_to * core, b_to * across + a_to * core
+
+    def device(a_to, b_to):
+        y_to, x_to = place(a_to, b_to)
+        return {"sp_1": y_to, "tp": 2 * x_to + core}
+
+    def slot(j, i):
+        y_at, x_at = place(ring_index(a, -j, na), ring_index(b, -i, na))
+        return rows_ref.at[y_at, x_at, core]
+
+    def one_copy(j, arriving):
+        ref = slot(0, j if arriving else 0)
+        return pltpu.make_async_remote_copy(
+            src_ref=ref, dst_ref=ref, send_sem=one_send.at[j], recv_sem=one_recv.at[j],
+            device_id=device(a, ring_index(b, j, na)), device_id_type=MESH,
+        )
+
+    def two_copy(j, i, arriving):
+        ref = slot(j if arriving else 0, i)
+        return pltpu.make_async_remote_copy(
+            src_ref=ref, dst_ref=ref, send_sem=two_send.at[j, i], recv_sem=two_recv.at[j, i],
+            device_id=device(ring_index(a, j, na), b), device_id_type=MESH,
+        )
+
+    partner = {"tp": t + 1 - 2 * core}
+
+    def pair_copy(j, i, arriving):
+        if arriving:
+            y_at, x_at = place(ring_index(a, -i, na), ring_index(b, -j, na))
+            ref = rows_ref.at[y_at, x_at, 1 - core]
+        else:
+            ref = slot(j, i)
+        return pltpu.make_async_remote_copy(
+            src_ref=ref, dst_ref=ref, send_sem=pair_send.at[j, i], recv_sem=pair_recv.at[j, i],
+            device_id=partner, device_id_type=MESH,
+        )
+
+    for j in range(1, na):
+        one_copy(j, False).start()
+    for j in range(1, na):
+        two_copy(j, 0, False).start()
+    pair_copy(0, 0, False).start()
+    for i in range(1, na):
+        one_copy(i, True).wait_recv()
+        for j in range(1, na):
+            two_copy(j, i, False).start()
+        pair_copy(0, i, False).start()
+    ring_steps(len(pending))
+    units_at = iota((taps_ref.shape[1], units), 0) == iota((taps_ref.shape[1], units), 1) + y * units
+    taps = exact(taps_ref[...], jnp.where(units_at, 1.0, 0.0))
+    for i in range(na):
+        for j in range(1, na):
+            two_copy(j, i, True).wait_recv()
+            pair_copy(j, i, False).start()
+    for i in range(na):
+        for j in range(na):
+            pair_copy(j, i, True).wait_recv()
+
+    tokens = na * n
+    rows_all = rows_ref[...].reshape(tokens, width)
+    gate_pre = plain(rows_all, full_ref[0], NT).astype(bf16)
+    edge = edge_out.shape[0]
+    edge_out[...] = gate_pre[tokens - edge :, :]
+
+    def edge_copy():
+        return pltpu.make_async_remote_copy(
+            src_ref=edge_out, dst_ref=edge_in, send_sem=edge_send.at[0], recv_sem=edge_recv.at[0],
+            device_id=along_z(ring_index(z, 1, nz)), device_id_type=MESH,
+        )
+
+    @pl.when(z < nz - 1)
+    def _():
+        edge_copy().start()
+
+    gate_scr[edge:, :] = gate_pre.astype(f32)
+    up_part = plain(rows_all, full_ref[1], NT).astype(bf16)
+
+    @pl.when(z > 0)
+    def _():
+        edge_copy().wait_recv()
+        gate_scr[:edge, :] = edge_in[...].astype(f32)
+
+    @pl.when(z == 0)
+    def _():
+        gate_scr[:edge, :] = jnp.zeros((edge, units), f32)
+
+    count = taps_ref.shape[0]
+    conv = jnp.zeros((tokens, units), f32)
+    for tap in range(count):
+        start = edge - count + 1 + tap
+        conv = conv + taps[tap : tap + 1, :] * gate_scr[start : start + tokens, :]
+    hidden = (conv / (1.0 + jnp.exp(-conv)) * up_part.astype(f32)).astype(bf16)
+
+    def swap_copy(part):
+        return pltpu.make_async_remote_copy(
+            src_ref=partial.at[part, :, 1 - core], dst_ref=swapped.at[part],
+            send_sem=swap_send.at[part], recv_sem=swap_recv.at[part],
+            device_id=partner, device_id_type=MESH,
+        )
+
+    for part in range(ny):
+        product = plain(hidden[part * n : (part + 1) * n, :], full_ref[2]).astype(bf16)
+        partial[part] = product.reshape(nx, 2, own, width)
+        swap_copy(part).start()
+
+    def first_copy(j):
+        return pltpu.make_async_remote_copy(
+            src_ref=summed.at[ring_index(a, j, na)], dst_ref=first.at[j],
+            send_sem=first_send.at[j], recv_sem=first_recv.at[j],
+            device_id=device(ring_index(a, j, na), b), device_id_type=MESH,
+        )
+
+    for part in range(ny):
+        swap_copy(part).wait_recv()
+    for j in list(range(1, na)) + [0]:
+        a_to = ring_index(a, j, na)
+        for b_to in range(na):
+            y_at, x_at = place(a_to, b_to)
+            both = partial[y_at, x_at, core].astype(f32) + swapped[y_at, x_at].astype(f32)
+            summed[a_to, b_to] = both.astype(bf16)
+        if j > 0:
+            first_copy(j).start()
+
+    def last_copy(j):
+        return pltpu.make_async_remote_copy(
+            src_ref=second.at[ring_index(b, j, na)], dst_ref=final.at[j],
+            send_sem=last_send.at[j], recv_sem=last_recv.at[j],
+            device_id=device(a, ring_index(b, j, na)), device_id_type=MESH,
+        )
+
+    for j in range(1, na):
+        first_copy(j).wait_recv()
+    for j in list(range(1, na)) + [0]:
+        b_to = ring_index(b, j, na)
+        total_rows = summed[a, b_to].astype(f32)
+        for i in range(1, na):
+            total_rows = total_rows + first[i, b_to].astype(f32)
+        second[b_to] = total_rows.astype(bf16)
+        if j > 0:
+            last_copy(j).start()
+    projected = second[b].astype(f32)
+    for j in range(1, na):
+        last_copy(j).wait_recv()
+    for j in range(1, na):
+        projected = projected + final[j].astype(f32)
+    out_ref[...] = (stream_ref[...] + projected).astype(bf16)
 
     for j in range(1, ny):
         near_copy(y, j).wait_send()
@@ -325,29 +516,46 @@
             plus_copy(c, s, ring_index(z, -s, nz)).wait_send()
         for s in range(n_minus):
             minus_copy(c, s, ring_index(z, s, nz)).wait_send()
-
-
-def mixer_and_weights(r, k, v, fade, rate, switch, bonus, rescale, gate, up, down):
-    nz, ny = lax.axis_size("sp_0"), lax.axis_size("sp_1")
+    for j in range(1, nt):
+        exit_copy(j).wait_send()
+    for j in range(1, na):
+        one_copy(j, False).wait_send()
+        first_copy(j).wait_send()
+        last_copy(j).wait_send()
+        for i in range(na):
+            two_copy(j, i, False).wait_send()
+    for i in range(na):
+        for j in range(na):
+            pair_copy(j, i, False).wait_send()
+    for part in range(ny):
+        swap_copy(part).wait_send()
+
+    @pl.when(z < nz - 1)
+    def _():
+        edge_copy().wait_send()
+
+
+def layer(r, k, v, fade, rate, switch, bonus, rescale, leave, skip, scaling, gate, up, taps, down):
+    nz, ny, nt = lax.axis_size("sp_0"), lax.axis_size("sp_1"), lax.axis_size("tp")
     span = min(4, nz)
     groups = nz // span
+    nx = nt // 2
     n = r.shape[0]
     rows, hidden = gate.shape
     units = hidden // ny
     wide = -(-units // 128) * 128
+    own, width = skip.shape
     dma = pltpu.SemaphoreType.DMA
-    block = pltpu.VMEM((n, n), bf16)
     in_vmem = pl.BlockSpec(memory_space=pltpu.VMEM)
     n_plus = nz // 2
+    edge = 16
     return pl.pallas_call(
-        functools.partial(mixer_kernel, nz, ny, span),
-        out_shape=(
-            jax.ShapeDtypeStruct((n, n), bf16),
-            jax.ShapeDtypeStruct((3, units, nz * ny * rows), bf16),
-        ),
-        in_specs=[in_vmem] * 11,
-        out_specs=(in_vmem, in_vmem),
+        functools.partial(layer_kernel, nz, ny, nt, span),
+        out_shape=jax.ShapeDtypeStruct((own, width), bf16),
+        in_specs=[in_vmem] * 15,
+        out_specs=in_vmem,
         scratch_shapes=[
+            pltpu.VMEM((3, units, nz * ny * rows), bf16),
             pltpu.VMEM((ny, n, n), bf16),
             pltpu.VMEM((span, n, n), bf16),
             pltpu.VMEM((groups, n, n), bf16),
@@ -357,57 +565,41 @@
             pltpu.VMEM((n, n), f32),
             pltpu.VMEM((4, n, n), f32),
             pltpu.VMEM((n, n), f32),
+            pltpu.VMEM((nt, own, width), bf16),
+            pltpu.VMEM((nt, own, width), bf16),
+            pltpu.VMEM((own, width), f32),
+            pltpu.VMEM((ny, nx, 2, own, width), bf16),
+            pltpu.VMEM((edge + ny * n, units), f32),
+            pltpu.VMEM((edge, units), bf16),
+            pltpu.VMEM((edge, units), bf16),
+            pltpu.VMEM((ny, nx, 2, own, width), bf16),
+            pltpu.VMEM((ny, nx, own, width), bf16),
+            pltpu.VMEM((ny, nx, own, width), bf16),
+            pltpu.VMEM((ny, nx, own, width), bf16),
+            pltpu.VMEM((nx, own, width), bf16),
+            pltpu.VMEM((nx, own, width), bf16),
             dma((ny,)), dma((ny,)), dma((span,)), dma((span,)), dma((groups,)), dma((groups,)),
             dma((ny,)), dma((ny,)),
             dma((3, n_plus)), dma((3, n_plus)), dma((3, n_plus)), dma((3, n_plus)),
+            dma((nt,)), dma((nt,)), dma((nx,)), dma((nx,)),
+            dma((ny, nx)), dma((ny, nx)), dma((ny, nx)), dma((ny, nx)),
+            dma((1,)), dma((1,)), dma((ny,)), dma((ny,)),
+            dma((ny,)), dma((ny,)), dma((nx,)), dma((nx,)),
         ],
-        compiler_params=pltpu.CompilerParams(collective_id=0, has_side_effects=True),
-        cost_estimate=pl.CostEstimate(flops=2 * 10**9, bytes_accessed=4 * 10**6, transcendentals=0),
-        name="mixer",
-    )(r, k, v, fade, rate, switch, bonus, rescale, gate, up, down)
-
-
-def in_blocks(shard, count):
-    return shard.reshape(count, -1, shard.shape[1])
-
-
-def summed_on_arrival(shard, axis):
-    count = lax.axis_size(axis)
-    tiles = lax.all_to_all(in_blocks(shard, count), axis, 0, 0, tiled=True)
-    return jnp.sum(tiles.astype(f32), axis=0)
+        compiler_params=pltpu.CompilerParams(
+            collective_id=0, has_side_effects=True, vmem_limit_bytes=48 * 2**20
+        ),
+        name="layer",
+    )(r, k, v, fade, rate, switch, bonus, rescale, leave, skip, scaling, gate, up, taps, down)
 
 
 def body(
-    r, k, v, fade, rate, switch, bonus, rescale, exit_weights, skip, scaling, gate, up, taps, down
+    r, k, v, fade, rate, switch, bonus, rescale, leave, skip, scaling, gate, up, taps, down
 ):
-    nz = lax.axis_size("sp_0")
-    mixed, weights = mixer_and_weights(
-        r, k, v, fade, rate, switch, bonus[None], rescale[None], gate, up, down
+    return layer(
+        r, k, v, fade, rate, switch, bonus[None], rescale[None], leave, skip, scaling[None],
+        gate, up, taps, down,
     )
-    attended = summed_on_arrival(
-        jnp.dot(mixed, exit_weights, preferred_element_type=f32).astype(bf16), "tp"
-    )
-    hidden_res = skip.astype(f32) + attended
-    normed = (
-        hidden_res
-        * lax.rsqrt(jnp.mean(hidden_res * hidden_res, axis=-1, keepdims=True) + norm_eps)
-        * scaling
-    ).astype(bf16)
-    rows = lax.all_gather(normed, ("sp_1", "tp"), tiled=True)
-    gate_pre = plain(rows, weights[0], NT).astype(bf16)
-    up_part = plain(rows, weights[1], NT).astype(bf16)
-    count = taps.shape[0]
-    units = gate_pre.shape[1]
-    route = [(i, i + 1) for i in range(nz - 1)]
-    tail = lax.ppermute(gate_pre[gate_pre.shape[0] - count + 1 :], "sp_0", route)
-    mine = lax.dynamic_slice_in_dim(taps, lax.axis_index("sp_1") * units, units, axis=1)
-    extended = jnp.concatenate([tail, gate_pre], axis=0).astype(f32)
-    conv = jnp.zeros(gate_pre.shape, f32)
-    for tap in range(count):
-        conv = conv + mine[tap] * extended[tap : tap + gate_pre.shape[0]]
-    hidden = (jax.nn.silu(conv) * up_part.astype(f32)).astype(bf16)
-    projected = summed_on_arrival(plain(hidden, weights[2]).astype(bf16), ("sp_1", "tp"))
-    return (hidden_res + projected).astype(bf16)
 
 
 def solution(mesh):

time: 193 us -> 96.4 us (0.50)
  the two profiles are of different devices: /device:TPU:1 before, /device:TPU:16 now
where the time goes in v2:
time: 96.4 us; the launch traced here: 95.7 us
  Pallas kernels  87.6 us (91%)
  local copies, waits for them, and re-layouts  8 us (8%)
    pallas_call x1, Pallas kernels, layer(): pl.pallas_call(functools.partial(layer_kernel, nz, ny, nt, span), out_sha...  87.6 us
    unnamed x30, local copies, waits for them, and re-layouts  8 us

profile of v2, /device:TPU:16, one launch (start us, length us, event | category | flops | bytes accessed | tf_op | source)
XLA Modules:
  0.0 95.7 jit_solution(14457819308028541942)
XLA Ops:
  0.0 0.0 copy-start.12
  0.0 0.0 copy-start.13
  0.0 0.0 copy-start.1
  0.0 0.0 copy-start.2
  0.0 0.0 copy-start.3
  0.0 0.0 copy-start.6
  0.0 1.0 %copy.16.down_ref = bf16[704,32]{1,0:T(8,128)(2,1)S(1)} copy(bf16[704,32]{0,1:T(8,128)(2,1)} %param.29) | data formatting | bytes 90112 | tf_op args[14]
  1.1 0.0 copy-done.12
  1.1 0.0 copy-done.13
  1.1 0.0 copy-done.1
  1.1 0.0 copy-done.2
  1.1 0.0 copy-done.3
  1.1 0.0 copy-done.6
  1.1 0.0 copy-start
  1.1 1.0 %copy-done = bf16[128,2048]{1,0:T(8,128)(2,1)S(1)} copy-done((bf16[128,2048]{1,0:T(8,128)(2,1)S(1)}, bf16[128,2048]{1,0:T(8,128)(2,1)}, u32[]{:S(2)}) %copy-start) | copy-done | bytes 524312
  2.2 0.0 copy-start.4
  2.2 0.8 copy-done.4
  3.0 0.0 copy-start.5
  3.0 0.8 copy-done.5
  3.8 0.0 copy-start.7
  3.8 0.8 copy-done.7
  4.5 0.0 copy-start.8
  4.5 0.8 copy-done.8
  5.3 0.0 copy-start.9
  5.3 0.8 copy-done.9
  6.1 0.0 copy-start.10
  6.1 0.7 copy-done.10
  6.8 0.0 copy-start.11
  6.8 0.7 copy-done.11
  7.5 87.6 %layer.1 = bf16[16,2048]{1,0:T(8,128)(2,1)S(1)} custom-call(bf16[128,128]{1,0:T(8,128)(2,1)S(1)} %copy-done.6, bf16[128,128]{1,0:T(8,128)(2,1)S(1)} %copy-done.7, bf16[128,128]{1,0:T(8,128)(2,1)S(1)} %copy-done.8, f32[128,128]{1,0:T(8,128)S(1)} %copy-done.1, f32[128,128]{1,0:T(8,128)S(1)} %copy-done.2, bf16[128,128]{1,0:T(8,128)(2,1)S(1)} %copy-done.9, ...), custom_call_target="tpu_custom_call" | custom-call | tf_op jit(solution)/shard_map/layer/pallas_call | solution.py:552
  95.1 0.6 copy.18
Async XLA Ops:
  0.0 1.1 %copy-start.12 = (f32[128]{0:T(128)S(1)}, f32[128]{0:T(128)}, u32[]{:S(2)}) copy-start(f32[128]{0:T(128)} %param.21) | copy-start | bytes 1540
  0.0 1.1 %copy-start.13 = (f32[128]{0:T(128)S(1)}, f32[128]{0:T(128)}, u32[]{:S(2)}) copy-start(f32[128]{0:T(128)} %param.22) | copy-start | bytes 1540
  0.0 1.1 %copy-start.1 = (f32[128,128]{1,0:T(8,128)S(1)}, f32[128,128]{1,0:T(8,128)}, u32[]{:S(2)}) copy-start(f32[128,128]{1,0:T(8,128)} %fade_ref.1) | copy-start | bytes 196612
  0.0 1.1 %copy-start.2 = (f32[128,128]{1,0:T(8,128)S(1)}, f32[128,128]{1,0:T(8,128)}, u32[]{:S(2)}) copy-start(f32[128,128]{1,0:T(8,128)} %rate_ref.1) | copy-start | bytes 196612
  0.0 1.1 %copy-start.3 = (bf16[16,2048]{1,0:T(8,128)(2,1)S(1)}, bf16[16,2048]{1,0:T(8,128)(2,1)}, u32[]{:S(2)}) copy-start(bf16[16,2048]{1,0:T(8,128)(2,1)} %skip_ref.1) | copy-start | bytes 196612
  0.0 1.1 %copy-start.6 = (bf16[128,128]{1,0:T(8,128)(2,1)S(1)}, bf16[128,128]{1,0:T(8,128)(2,1)}, u32[]{:S(2)}) copy-start(bf16[128,128]{1,0:T(8,128)(2,1)} %r_ref.1) | copy-start | bytes 98308
  1.1 1.0 %copy-start = (bf16[128,2048]{1,0:T(8,128)(2,1)S(1)}, bf16[128,2048]{1,0:T(8,128)(2,1)}, u32[]{:S(2)}) copy-start(bf16[128,2048]{1,0:T(8,128)(2,1)} %exit_ref.1) | copy-start | bytes 1572868
  2.2 0.8 copy-start.4
  3.0 0.8 copy-start.5
  3.8 0.8 copy-start.7
  4.5 0.8 copy-start.8
  5.3 0.8 copy-start.9
  6.1 0.7 copy-start.10
  6.8 0.7 copy-start.11

commit v3 on v2

--- a/solution.py
+++ b/solution.py
@@ -12,6 +12,9 @@
 SP = ("sp_0", "sp_1")
 SP_TP = ("sp_0", "sp_1", "tp")
 COLUMNS = 4
+BANDS = 4
+SPLIT = 16
+FIRST, SECOND, MIDDLE, LATE = 1, 2, 2, 1
 MESH = pl.DeviceIdType.MESH
 
 group_eps = 0.00064
@@ -32,6 +35,30 @@
 
 def plain(a, b, dims=NN):
     return lax.dot_general(a, b, dims, preferred_element_type=f32)
+
+
+def split(a):
+    high = a.astype(bf16)
+    return high, (a - high.astype(f32)).astype(bf16)
+
+
+def fine(a, b, dims=NN):
+    (a_dim,), (b_dim,) = dims[0]
+    a_high, a_low = split(a)
+    b_high, b_low = split(b)
+    left = jnp.concatenate([a_high, a_high, a_low], axis=a_dim)
+    right = jnp.concatenate([b_high, b_low, b_high], axis=b_dim)
+    return plain(left, right, dims)
+
+
+def left_exact(a, b):
+    a = a.astype(bf16)
+    return plain(jnp.concatenate([a, a], axis=1), jnp.concatenate(split(b), axis=0))
+
+
+def right_exact(a, b):
+    b = b.astype(bf16)
+    return plain(jnp.concatenate(split(a), axis=1), jnp.concatenate([b, b], axis=0))
 
 
 def iota(shape, dim):
@@ -62,7 +89,7 @@
 
 
 def compose(earlier, latter):
-    both = exact(latter[0], jnp.concatenate(earlier, axis=1))
+    both = left_exact(latter[0], jnp.concatenate(earlier, axis=1))
     n = 2 * WIDTH
     return both[:, :n], both[:, n:] + latter[1]
 
@@ -79,26 +106,27 @@
     return before, total
 
 
-def block_inverse(strict):
+def block_inverse(strict, found, first, end):
     n = strict.shape[0]
     row, col = iota((n, n), 0), iota((n, n), 1)
-    found = jnp.where(row == col, 1.0, 0.0) + jnp.where(row // 2 == col // 2, strict, 0.0)
-    m = 2
-    while m < n:
+    if found is None:
+        found = jnp.where(row == col, 1.0, 0.0) + jnp.where(row // 2 == col // 2, strict, 0.0)
+    m = first
+    while m < end:
         edge = jnp.where((row // (2 * m) == col // (2 * m)) & (row // m != col // m), strict, 0.0)
-        found = found + exact(found, exact(edge, found))
+        found = found + fine(found, fine(edge, found))
         m *= 2
     return found
 
 
-def local_mixer(r_ref, k_ref, v_ref, fade_ref, rate_ref):
+def mixer_start(r_ref, k_ref, v_ref, fade_ref, rate_ref):
     r, k, v = r_ref[...].astype(f32), k_ref[...].astype(f32), v_ref[...].astype(f32)
     n = r.shape[0]
     row, col = iota((n, n), 0), iota((n, n), 1)
     ones = jnp.where(head_blocks(n), 1.0, 0.0)
     log_fade = -jax.nn.sigmoid(fade_ref[...]) * 0.6065306597126334
-    total_log = exact(jnp.where(row >= col, 1.0, 0.0), log_fade)
-    length = jnp.sqrt(exact(k * k, ones))
+    total_log = left_exact(jnp.where(row >= col, 1.0, 0.0), log_fade)
+    length = jnp.sqrt(right_exact(k * k, ones))
     unit = k / jnp.maximum(length, 1.0)
     amount = unit * jax.nn.sigmoid(rate_ref[...])
     kept = jnp.exp(total_log)
@@ -108,43 +136,68 @@
     amount_grown, key_grown = amount * grown, k * grown
     last = kept[n - 1 :, :]
     right = jnp.concatenate([amount_grown, key_grown], axis=0)
+    heads = []
+    for h in range(n // WIDTH):
+        mine = col // WIDTH == h
+        erase_h = jnp.where(mine, erase, 0.0)
+        read_h = jnp.where(mine, read, 0.0)
+        grams = fine(jnp.concatenate([erase_h, read_h], axis=0), right, NT)
+        within = jnp.where(row > col, grams[:n, :n], 0.0)
+        heads.append((erase_h, grams, within, block_inverse(within, None, 2, SPLIT)))
+    return v, read, last, amount_grown, key_grown, heads
+
+
+def mixer_end(v, read, last, amount_grown, key_grown, heads):
+    n = v.shape[0]
+    row, col = iota((n, n), 0), iota((n, n), 1)
     strict, lower = row > col, row >= col
     maps = jnp.zeros((n, n), f32)
     values = jnp.zeros((n, n), f32)
     probe, local_out = read, jnp.zeros((n, n), f32)
-    for h in range(n // WIDTH):
-        mine = col // WIDTH == h
-        erase_h = jnp.where(mine, erase, 0.0)
-        read_h = jnp.where(mine, read, 0.0)
-        value_h = jnp.where(mine, v, 0.0)
-        grams = exact(jnp.concatenate([erase_h, read_h], axis=0), right, NT)
-        inverse = block_inverse(jnp.where(strict, grams[:n, :n], 0.0))
-        pushed = exact(jnp.where(strict, grams[:n, n:], 0.0), value_h)
-        solved = exact(inverse, jnp.concatenate([erase_h, pushed], axis=1))
-        shown = exact(jnp.where(lower, grams[n:, :n], 0.0), solved)
+    for h, (erase_h, grams, within, inverse) in enumerate(heads):
+        value_h = jnp.where(col // WIDTH == h, v, 0.0)
+        inverse = block_inverse(within, inverse, SPLIT, n)
+        pushed = fine(jnp.where(strict, grams[:n, n:], 0.0), value_h)
+        solved = fine(inverse, jnp.concatenate([erase_h, pushed], axis=1))
+        shown = fine(jnp.where(lower, grams[n:, :n], 0.0), solved)
         local_out = local_out + shown[:, n:]
-        local_out = local_out + exact(jnp.where(lower, grams[n:, n:], 0.0), value_h)
+        local_out = local_out + fine(jnp.where(lower, grams[n:, n:], 0.0), value_h)
         probe = probe + shown[:, :n]
         maps = maps + solved[:, :n]
         values = values + solved[:, n:]
     same = head_blocks(n)
     amount_end, key_end = amount_grown * last, key_grown * last
-    mapping = jnp.where(row == col, last, 0.0) + jnp.where(same, exact(amount_end, maps, TN), 0.0)
-    state = jnp.where(same, exact(amount_end, values, TN) + exact(key_end, v, TN), 0.0)
+    mapping = jnp.where(row == col, last, 0.0) + jnp.where(same, fine(amount_end, maps, TN), 0.0)
+    state = jnp.where(same, fine(amount_end, values, TN) + fine(key_end, v, TN), 0.0)
     return mapping, state, probe, local_out
 
 
 def layer_kernel(
-    nz, ny, nt, span, r_ref, k_ref, v_ref, fade_ref, rate_ref, switch_ref, bonus_ref, rescale_ref,
-    exit_ref, skip_ref, scaling_ref, gate_ref, up_ref, taps_ref, down_ref, out_ref,
+    nz, ny, nt, span, inputs, *refs,
+):
+    given, out_ref, held = refs[:inputs], refs[inputs], refs[inputs + 1 : 2 * inputs + 1]
+    load_sem, rest = refs[2 * inputs + 1], refs[2 * inputs + 2 :]
+    (
+        r_ref, k_ref, v_ref, fade_ref, rate_ref, switch_ref, bonus_ref, rescale_ref,
+        exit_ref, skip_ref, scaling_ref, gate_ref, up_ref, taps_ref, down_ref,
+    ) = held
+    loads = [
+        pltpu.make_async_copy(source, target, load_sem.at[i])
+        for i, (source, target) in enumerate(zip(given, held))
+    ]
+    first_loads, second_loads = [3, 1, 4, 0, 2], [11, 12, 14]
+    last_loads = [i for i in range(inputs) if i not in first_loads + second_loads]
+    for i in first_loads + second_loads + last_loads:
+        loads[i].start()
+    (
     full_ref, near, mid, far, pieces, parts, probe_ref, local_ref, before_ref, carry_ref,
     sent, landed, stream_ref, rows_ref, gate_scr, edge_out, edge_in, partial, swapped, summed,
-    first, second, final,
-    near_send, near_recv, mid_send, mid_recv, far_send, far_recv, part_send, part_recv,
+    first, second, final, gate_rows_ref, up_rows_ref,
+    token_sem, near_send, near_recv, mid_send, mid_recv, far_send, far_recv, part_send, part_recv,
     plus_send, plus_recv, minus_send, minus_recv,
     exit_send, exit_recv, one_send, one_recv, two_send, two_recv, pair_send, pair_recv,
     edge_send, edge_recv, swap_send, swap_recv, first_send, first_recv, last_send, last_recv,
-):
+    ) = rest
     z, y, t = lax.axis_index("sp_0"), lax.axis_index("sp_1"), lax.axis_index("tp")
     nx = nt // 2
     x, core = t // 2, lax.rem(t, 2)
@@ -163,7 +216,8 @@
     barrier = pltpu.get_barrier_semaphore()
     for j in range(1, ny):
         pl.semaphore_signal(barrier, inc=1, device_id=along_y(j), device_id_type=MESH)
-    for j in range(1, nz):
+    reach = sorted({j % nz for j in range(-span, span + 1)} - {0})
+    for j in reach:
         pl.semaphore_signal(
             barrier, inc=1, device_id=along_z(ring_index(z, j, nz)), device_id_type=MESH
         )
@@ -172,14 +226,13 @@
             barrier, inc=1, device_id={"tp": ring_index(t, j, nt)}, device_id_type=MESH
         )
 
-    mapping, state, probe, local_out = local_mixer(r_ref, k_ref, v_ref, fade_ref, rate_ref)
-    near[y] = packed(mapping, state)
-    probe_ref[...] = probe
-    local_ref[...] = local_out
-
-    eye = jnp.where(iota((rows, rows), 0) == iota((rows, rows), 1), 1.0, 0.0).astype(bf16)
-    down_turned = plain(eye, down_ref[...], NT).astype(bf16)
-    stacked = jnp.concatenate([gate_ref[...], up_ref[...], down_turned], axis=0)
+    for i in first_loads:
+        loads[i].wait()
+    begun = mixer_start(r_ref, k_ref, v_ref, fade_ref, rate_ref)
+
+    for i in second_loads:
+        loads[i].wait()
+    stacked = jnp.concatenate([gate_ref[...], up_ref[...], down_ref[...]], axis=0)
     wide = pieces.shape[2]
     tall = stacked.shape[1]
     for part in range(ny):
@@ -187,7 +240,13 @@
         pick = jnp.where((at == to + part * units) & (to < units), 1.0, 0.0).astype(bf16)
         pieces[part] = plain(stacked, pick).astype(bf16)
 
-    pl.semaphore_wait(barrier, ny - 1 + nz - 1 + nt - 1)
+    for i in last_loads:
+        loads[i].wait()
+    pl.semaphore_wait(barrier, ny - 1 + len(reach) + nt - 1)
+    if nz > 2 * span:
+        pl.semaphore_signal(
+            token_sem, inc=1, device_id=along_z(ring_index(z, -span, nz)), device_id_type=MESH
+        )
 
     def near_copy(source, target):
         return pltpu.make_async_remote_copy(
@@ -206,28 +265,15 @@
         )
 
     for j in range(1, ny):
-        near_copy(y, j).start()
-    for j in range(1, ny):
         part_copy(j, False).start()
     parts[y] = pieces[y]
 
+    mapping, state, probe, local_out = mixer_end(*begun)
+    near[y] = packed(mapping, state)
     for j in range(1, ny):
-        near_copy(ring_index(y, -j, ny), j).wait_recv()
-    before, total = folded(near, ny, y)
-    before_ref[0] = before[0]
-    before_ref[1] = before[1]
-
-    def mid_copy(source, j):
-        to = z - inner + ring_index(inner, j, span)
-        return pltpu.make_async_remote_copy(
-            src_ref=mid.at[source], dst_ref=mid.at[source],
-            send_sem=mid_send.at[j], recv_sem=mid_recv.at[j],
-            device_id=along_z(to), device_id_type=MESH,
-        )
-
-    mid[inner] = packed(*total)
-    for j in range(1, span):
-        mid_copy(inner, j).start()
+        near_copy(y, j).start()
+    probe_ref[...] = probe
+    local_ref[...] = local_out
 
     for j in range(1, ny):
         part_copy(j, True).wait_recv()
@@ -271,7 +317,32 @@
                 minus_copy(c, s, ring_index(z, s, nz)).start()
 
     ring_step(0)
-
+    pending = list(range(1, n_plus + 1))
+
+    def ring_steps(count):
+        for s in pending[:count]:
+            ring_step(s)
+        del pending[:count]
+
+    for j in range(1, ny):
+        near_copy(ring_index(y, -j, ny), j).wait_recv()
+    before, total = folded(near, ny, y)
+    before_ref[0] = before[0]
+    before_ref[1] = before[1]
+
+    def mid_copy(source, j):
+        to = z - inner + ring_index(inner, j, span)
+        return pltpu.make_async_remote_copy(
+            src_ref=mid.at[source], dst_ref=mid.at[source],
+            send_sem=mid_send.at[j], recv_sem=mid_recv.at[j],
+            device_id=along_z(to), device_id_type=MESH,
+        )
+
+    mid[inner] = packed(*total)
+    for j in range(1, span):
+        mid_copy(inner, j).start()
+
+    ring_steps(FIRST)
     for j in range(1, span):
         mid_copy(ring_index(inner, -j, span), j).wait_recv()
     before_z, total_z = folded(mid, span, inner)
@@ -286,15 +357,14 @@
         )
 
     far[outer] = packed(*total_z)
+    if nz > 2 * span:
+        pl.semaphore_wait(token_sem, 1)
     for d in range(1, groups):
         @pl.when(outer + d < groups)
         def _():
             far_copy(outer, d, lax.rem(z + d * span, nz)).start()
 
-    steps = n_plus + 1
-    early = min(3, steps - 1)
-    for s in range(1, 1 + early):
-        ring_step(s)
+    ring_steps(SECOND)
 
     carry_ref[...] = jnp.zeros((n, n), f32)
     for g in range(groups - 1):
@@ -305,25 +375,19 @@
                 def _():
                     far_copy(g, d, lax.rem(z + d * span, nz)).wait_recv()
             step = unpacked(far[g])
-            carry_ref[...] = exact(step[0], carry_ref[...]) + step[1]
-    incoming = exact(before_ref[2], carry_ref[...]) + before_ref[3]
-    incoming = exact(before_ref[0], incoming) + before_ref[1]
-
-    closing = local_ref[...] + exact(probe_ref[...], incoming)
+            carry_ref[...] = left_exact(step[0], carry_ref[...]) + step[1]
+    incoming = fine(before_ref[2], carry_ref[...]) + before_ref[3]
+    incoming = fine(before_ref[0], incoming) + before_ref[1]
+
+    closing = local_ref[...] + fine(probe_ref[...], incoming)
     ones = jnp.where(head_blocks(n), 1.0, 0.0)
-    centred = closing - exact(closing, ones) * (1.0 / WIDTH)
-    spread = exact(centred * centred, ones) * (1.0 / WIDTH)
+    centred = closing - right_exact(closing, ones) * (1.0 / WIDTH)
+    spread = right_exact(centred * centred, ones) * (1.0 / WIDTH)
     rescaled = centred * lax.rsqrt(spread + group_eps) * rescale_ref[...]
     value = v_ref[...].astype(f32)
-    bonus = exact(r_ref[...].astype(f32) * k_ref[...].astype(f32) * bonus_ref[...], ones) * value
+    bonus = right_exact(r_ref[...].astype(f32) * k_ref[...].astype(f32) * bonus_ref[...], ones)
+    bonus = bonus * value
     mixed = ((rescaled + bonus) * switch_ref[...].astype(f32)).astype(bf16)
-
-    pending = list(range(1 + early, steps))
-
-    def ring_steps(count):
-        for s in pending[:count]:
-            ring_step(s)
-        del pending[:count]
 
     own = n // nt
     width = exit_ref.shape[1]
@@ -339,7 +403,7 @@
     sent[...] = plain(mixed, exit_ref[...]).astype(bf16).reshape(nt, own, width)
     for j in range(1, nt):
         exit_copy(j).start()
-    ring_steps(2)
+    ring_steps(MIDDLE)
     attended = sent[t].astype(f32)
     for j in range(1, nt):
         exit_copy(j).wait_recv()
@@ -397,6 +461,7 @@
     for j in range(1, na):
         two_copy(j, 0, False).start()
     pair_copy(0, 0, False).start()
+    ring_steps(LATE)
     for i in range(1, na):
         one_copy(i, True).wait_recv()
         for j in range(1, na):
@@ -409,13 +474,20 @@
         for j in range(1, na):
             two_copy(j, i, True).wait_recv()
             pair_copy(j, i, False).start()
+    tokens = na * n
+    half = tokens // 2
+
+    def projections(c):
+        rows = rows_ref[:, :, c].reshape(half, width)
+        gate_rows_ref[:, :, c] = plain(rows, full_ref[0], NT).reshape(ny, nx, own, units)
+        up_rows_ref[:, :, c] = plain(rows, full_ref[1], NT).reshape(ny, nx, own, units)
+
+    projections(core)
     for i in range(na):
         for j in range(na):
             pair_copy(j, i, True).wait_recv()
-
-    tokens = na * n
-    rows_all = rows_ref[...].reshape(tokens, width)
-    gate_pre = plain(rows_all, full_ref[0], NT).astype(bf16)
+    projections(1 - core)
+    gate_pre = gate_rows_ref[...].reshape(tokens, units).astype(bf16)
     edge = edge_out.shape[0]
     edge_out[...] = gate_pre[tokens - edge :, :]
 
@@ -430,7 +502,7 @@
         edge_copy().start()
 
     gate_scr[edge:, :] = gate_pre.astype(f32)
-    up_part = plain(rows_all, full_ref[1], NT).astype(bf16)
+    up_part = up_rows_ref[...].reshape(tokens, units).astype(bf16)
 
     @pl.when(z > 0)
     def _():
@@ -448,59 +520,65 @@
         conv = conv + taps[tap : tap + 1, :] * gate_scr[start : start + tokens, :]
     hidden = (conv / (1.0 + jnp.exp(-conv)) * up_part.astype(f32)).astype(bf16)
 
-    def swap_copy(part):
-        return pltpu.make_async_remote_copy(
-            src_ref=partial.at[part, :, 1 - core], dst_ref=swapped.at[part],
-            send_sem=swap_send.at[part], recv_sem=swap_recv.at[part],
+    bands = partial.shape[0]
+    band = width // bands
+
+    def swap_copy(p):
+        return pltpu.make_async_remote_copy(
+            src_ref=partial.at[p, :, :, 1 - core], dst_ref=swapped.at[p],
+            send_sem=swap_send.at[p], recv_sem=swap_recv.at[p],
             device_id=partner, device_id_type=MESH,
         )
 
-    for part in range(ny):
-        product = plain(hidden[part * n : (part + 1) * n, :], full_ref[2]).astype(bf16)
-        partial[part] = product.reshape(nx, 2, own, width)
-        swap_copy(part).start()
-
-    def first_copy(j):
-        return pltpu.make_async_remote_copy(
-            src_ref=summed.at[ring_index(a, j, na)], dst_ref=first.at[j],
-            send_sem=first_send.at[j], recv_sem=first_recv.at[j],
+    def first_copy(p, j):
+        return pltpu.make_async_remote_copy(
+            src_ref=summed.at[p, ring_index(a, j, na)], dst_ref=first.at[p, j],
+            send_sem=first_send.at[p, j], recv_sem=first_recv.at[p, j],
             device_id=device(ring_index(a, j, na), b), device_id_type=MESH,
         )
 
-    for part in range(ny):
-        swap_copy(part).wait_recv()
-    for j in list(range(1, na)) + [0]:
-        a_to = ring_index(a, j, na)
-        for b_to in range(na):
-            y_at, x_at = place(a_to, b_to)
-            both = partial[y_at, x_at, core].astype(f32) + swapped[y_at, x_at].astype(f32)
-            summed[a_to, b_to] = both.astype(bf16)
-        if j > 0:
-            first_copy(j).start()
-
-    def last_copy(j):
-        return pltpu.make_async_remote_copy(
-            src_ref=second.at[ring_index(b, j, na)], dst_ref=final.at[j],
-            send_sem=last_send.at[j], recv_sem=last_recv.at[j],
+    def last_copy(p, j):
+        return pltpu.make_async_remote_copy(
+            src_ref=second.at[p, ring_index(b, j, na)], dst_ref=final.at[p, j],
+            send_sem=last_send.at[p, j], recv_sem=last_recv.at[p, j],
             device_id=device(a, ring_index(b, j, na)), device_id_type=MESH,
         )
 
-    for j in range(1, na):
-        first_copy(j).wait_recv()
-    for j in list(range(1, na)) + [0]:
-        b_to = ring_index(b, j, na)
-        total_rows = summed[a, b_to].astype(f32)
-        for i in range(1, na):
-            total_rows = total_rows + first[i, b_to].astype(f32)
-        second[b_to] = total_rows.astype(bf16)
-        if j > 0:
-            last_copy(j).start()
-    projected = second[b].astype(f32)
-    for j in range(1, na):
-        last_copy(j).wait_recv()
-    for j in range(1, na):
-        projected = projected + final[j].astype(f32)
-    out_ref[...] = (stream_ref[...] + projected).astype(bf16)
+    for p in range(bands):
+        product = plain(hidden, full_ref[2, :, p * band : (p + 1) * band]).astype(bf16)
+        partial[p] = product.reshape(ny, nx, 2, own, band)
+        swap_copy(p).start()
+    order = list(range(1, na)) + [0]
+    for p in range(bands):
+        swap_copy(p).wait_recv()
+        for j in order:
+            a_to = ring_index(a, j, na)
+            for b_to in range(na):
+                y_at, x_at = place(a_to, b_to)
+                both = partial[p, y_at, x_at, core].astype(f32)
+                both = both + swapped[p, y_at, x_at].astype(f32)
+                summed[p, a_to, b_to] = both.astype(bf16)
+            if j > 0:
+                first_copy(p, j).start()
+    for p in range(bands):
+        for j in range(1, na):
+            first_copy(p, j).wait_recv()
+        for j in order:
+            b_to = ring_index(b, j, na)
+            total_rows = summed[p, a, b_to].astype(f32)
+            for i in range(1, na):
+                total_rows = total_rows + first[p, i, b_to].astype(f32)
+            second[p, b_to] = total_rows.astype(bf16)
+            if j > 0:
+                last_copy(p, j).start()
+    for p in range(bands):
+        projected = second[p, b].astype(f32)
+        for j in range(1, na):
+            last_copy(p, j).wait_recv()
+        for j in range(1, na):
+            projected = projected + final[p, j].astype(f32)
+        columns = slice(p * band, (p + 1) * band)
+        out_ref[:, columns] = (stream_ref[:, columns] + projected).astype(bf16)
 
     for j in range(1, ny):
         near_copy(y, j).wait_send()
@@ -520,22 +598,24 @@
         exit_copy(j).wait_send()
     for j in range(1, na):
         one_copy(j, False).wait_send()
-        first_copy(j).wait_send()
-        last_copy(j).wait_send()
+        for p in range(bands):
+            first_copy(p, j).wait_send()
+            last_copy(p, j).wait_send()
         for i in range(na):
             two_copy(j, i, False).wait_send()
     for i in range(na):
         for j in range(na):
             pair_copy(j, i, False).wait_send()
-    for part in range(ny):
-        swap_copy(part).wait_send()
+    for p in range(bands):
+        swap_copy(p).wait_send()
 
     @pl.when(z < nz - 1)
     def _():
         edge_copy().wait_send()
 
 
-def layer(r, k, v, fade, rate, switch, bonus, rescale, leave, skip, scaling, gate, up, taps, down):
+def layer(*args):
+    r, skip, gate = args[0], args[9], args[11]
     nz, ny, nt = lax.axis_size("sp_0"), lax.axis_size("sp_1"), lax.axis_size("tp")
     span = min(4, nz)
     groups = nz // span
@@ -545,16 +625,19 @@
     units = hidden // ny
     wide = -(-units // 128) * 128
     own, width = skip.shape
+    band = width // BANDS
     dma = pltpu.SemaphoreType.DMA
     in_vmem = pl.BlockSpec(memory_space=pltpu.VMEM)
     n_plus = nz // 2
     edge = 16
     return pl.pallas_call(
-        functools.partial(layer_kernel, nz, ny, nt, span),
+        functools.partial(layer_kernel, nz, ny, nt, span, len(args)),
         out_shape=jax.ShapeDtypeStruct((own, width), bf16),
-        in_specs=[in_vmem] * 15,
+        in_specs=[pl.BlockSpec(memory_space=pl.ANY)] * len(args),
         out_specs=in_vmem,
-        scratch_shapes=[
+        scratch_shapes=[pltpu.VMEM(arg.shape, arg.dtype) for arg in args]
+        + [
+            dma((len(args),)),
             pltpu.VMEM((3, units, nz * ny * rows), bf16),
             pltpu.VMEM((ny, n, n), bf16),
             pltpu.VMEM((span, n, n), bf16),
@@ -572,25 +655,28 @@
             pltpu.VMEM((edge + ny * n, units), f32),
             pltpu.VMEM((edge, units), bf16),
             pltpu.VMEM((edge, units), bf16),
-            pltpu.VMEM((ny, nx, 2, own, width), bf16),
-            pltpu.VMEM((ny, nx, own, width), bf16),
-            pltpu.VMEM((ny, nx, own, width), bf16),
-            pltpu.VMEM((ny, nx, own, width), bf16),
-            pltpu.VMEM((nx, own, width), bf16),
-            pltpu.VMEM((nx, own, width), bf16),
+            pltpu.VMEM((BANDS, ny, nx, 2, own, band), bf16),
+            pltpu.VMEM((BANDS, ny, nx, own, band), bf16),
+            pltpu.VMEM((BANDS, ny, nx, own, band), bf16),
+            pltpu.VMEM((BANDS, ny, nx, own, band), bf16),
+            pltpu.VMEM((BANDS, nx, own, band), bf16),
+            pltpu.VMEM((BANDS, nx, own, band), bf16),
+            pltpu.VMEM((ny, nx, 2, own, units), f32),
+            pltpu.VMEM((ny, nx, 2, own, units), f32),
+            pltpu.SemaphoreType.REGULAR,
             dma((ny,)), dma((ny,)), dma((span,)), dma((span,)), dma((groups,)), dma((groups,)),
             dma((ny,)), dma((ny,)),
             dma((3, n_plus)), dma((3, n_plus)), dma((3, n_plus)), dma((3, n_plus)),
             dma((nt,)), dma((nt,)), dma((nx,)), dma((nx,)),
             dma((ny, nx)), dma((ny, nx)), dma((ny, nx)), dma((ny, nx)),
-            dma((1,)), dma((1,)), dma((ny,)), dma((ny,)),
-            dma((ny,)), dma((ny,)), dma((nx,)), dma((nx,)),
+            dma((1,)), dma((1,)), dma((BANDS,)), dma((BANDS,)),
+            dma((BANDS, ny)), dma((BANDS, ny)), dma((BANDS, nx)), dma((BANDS, nx)),
         ],
         compiler_params=pltpu.CompilerParams(
-            collective_id=0, has_side_effects=True, vmem_limit_bytes=48 * 2**20
+            collective_id=0, has_side_effects=True, vmem_limit_bytes=67043328
         ),
         name="layer",
-    )(r, k, v, fade, rate, switch, bonus, rescale, leave, skip, scaling, gate, up, taps, down)
+    )(*args)
 
 
 def body(
@@ -598,7 +684,7 @@
 ):
     return layer(
         r, k, v, fade, rate, switch, bonus[None], rescale[None], leave, skip, scaling[None],
-        gate, up, taps, down,
+        gate, up, taps, down.T,
     )
 
 

time: 96.4 us -> 84 us (0.87)
  the two profiles are of different devices: /device:TPU:16 before, /device:TPU:32 now
where the time goes in v3:
time: 84 us; the launch traced here: 83.8 us
  Pallas kernels  82.3 us (98%)
  local copies, waits for them, and re-layouts  1.47 us (2%)
    pallas_call x1, Pallas kernels, layer(): pl.pallas_call(functools.partial(layer_kernel, nz, ny, nt, span, len(args...  82.3 us

profile of v3, /device:TPU:32, one launch (start us, length us, event | category | flops | bytes accessed | tf_op | source)
XLA Modules:
  0.0 83.8 jit_solution(16214282802023782140)
XLA Ops:
  0.0 82.3 %layer.1 = bf16[16,2048]{1,0:T(8,128)(2,1)} custom-call(bf16[128,128]{1,0:T(8,128)(2,1)} %refs_0_.1, bf16[128,128]{1,0:T(8,128)(2,1)} %refs_1_.1, bf16[128,128]{1,0:T(8,128)(2,1)} %refs_2_.1, f32[128,128]{1,0:T(8,128)} %refs_3_.1, f32[128,128]{1,0:T(8,128)} %refs_4_.1, bf16[128,128]{1,0:T(8,128)(2,1)} %refs_5_.1, f32[1,128]{1,0:T(1,128)} %bitcast.6, ...), custom_call_target="tpu_custom_call" | custom-call | tf_op jit(solution)/shard_map/layer/pallas_call | solution.py:633
  82.3 1.5 %copy.17 = bf16[16,2048]{1,0:T(8,128)(2,1)} copy(bf16[16,2048]{1,0:T(8,128)(2,1)} %layer.1) | data formatting | bytes 131072

commit v4 on v3

--- a/solution.py
+++ b/solution.py
@@ -14,7 +14,7 @@
 COLUMNS = 4
 BANDS = 4
 SPLIT = 16
-FIRST, SECOND, MIDDLE, LATE = 1, 2, 2, 1
+MIX, LATER, LESS = 0, 2, 1
 MESH = pl.DeviceIdType.MESH
 
 group_eps = 0.00064
@@ -79,13 +79,13 @@
     ).astype(bf16)
 
 
+def unpacked_half(half):
+    half = half.astype(f32)
+    return jnp.where(head_blocks(2 * WIDTH), jnp.concatenate([half, half], axis=0), 0.0)
+
+
 def unpacked(block):
-    block = block.astype(f32)
-    same = head_blocks(2 * WIDTH)
-    mapping, state = block[:WIDTH], block[WIDTH:]
-    mapping = jnp.where(same, jnp.concatenate([mapping, mapping], axis=0), 0.0)
-    state = jnp.where(same, jnp.concatenate([state, state], axis=0), 0.0)
-    return mapping, state
+    return unpacked_half(block[:WIDTH]), unpacked_half(block[WIDTH:])
 
 
 def compose(earlier, latter):
@@ -94,15 +94,15 @@
     return both[:, :n], both[:, n:] + latter[1]
 
 
-def folded(slots, count, position):
+def folded(slots, heads, count, position):
     n = 2 * WIDTH
     eye = jnp.where(iota((n, n), 0) == iota((n, n), 1), 1.0, 0.0)
     before = (eye, jnp.zeros((n, n), f32))
-    total = unpacked(slots[0])
+    total = unpacked(slots[0, heads])
     for k in range(1, count):
         hit = position == k
         before = tuple(jnp.where(hit, new, old) for new, old in zip(total, before))
-        total = compose(total, unpacked(slots[k]))
+        total = compose(total, unpacked(slots[k, heads]))
     return before, total
 
 
@@ -190,11 +190,12 @@
     for i in first_loads + second_loads + last_loads:
         loads[i].start()
     (
-    full_ref, near, mid, far, pieces, parts, probe_ref, local_ref, before_ref, carry_ref,
+    full_ref, near, mid, far, pieces, parts, finish_ref, before_ref, carry_ref, exit_both,
     sent, landed, stream_ref, rows_ref, gate_scr, edge_out, edge_in, partial, swapped, summed,
     first, second, final, gate_rows_ref, up_rows_ref,
     token_sem, near_send, near_recv, mid_send, mid_recv, far_send, far_recv, part_send, part_recv,
     plus_send, plus_recv, minus_send, minus_recv,
+    finish_send, finish_recv, twin_send, twin_recv, hand_send, hand_recv,
     exit_send, exit_recv, one_send, one_recv, two_send, two_recv, pair_send, pair_recv,
     edge_send, edge_recv, swap_send, swap_recv, first_send, first_recv, last_send, last_recv,
     ) = rest
@@ -204,7 +205,7 @@
     groups = nz // span
     inner, outer = lax.rem(z, span), z // span
     n = 2 * WIDTH
-    units = full_ref.shape[1]
+    units = full_ref.shape[2]
     rows = gate_ref.shape[0]
 
     def along_y(j):
@@ -213,9 +214,20 @@
     def along_z(to):
         return {"sp_0": to}
 
+    mixes = core == MIX
+    forwards = core == 1 - MIX
+    head_set = jnp.where(mixes, 0, 1)
+    chip = t - core
+    mate = chip + 1 - core
+    mixer_at, ring_at = chip + MIX, chip + 1 - MIX
+
     barrier = pltpu.get_barrier_semaphore()
     for j in range(1, ny):
-        pl.semaphore_signal(barrier, inc=1, device_id=along_y(j), device_id_type=MESH)
+        for to in (t, mate):
+            pl.semaphore_signal(
+                barrier, inc=1, device_id={"sp_1": ring_index(y, j, ny), "tp": to},
+                device_id_type=MESH,
+            )
     reach = sorted({j % nz for j in range(-span, span + 1)} - {0})
     for j in reach:
         pl.semaphore_signal(
@@ -242,93 +254,155 @@
 
     for i in last_loads:
         loads[i].wait()
-    pl.semaphore_wait(barrier, ny - 1 + len(reach) + nt - 1)
+    pl.semaphore_wait(barrier, 2 * (ny - 1) + len(reach) + nt - 1)
     if nz > 2 * span:
         pl.semaphore_signal(
             token_sem, inc=1, device_id=along_z(ring_index(z, -span, nz)), device_id_type=MESH
         )
 
-    def near_copy(source, target):
-        return pltpu.make_async_remote_copy(
-            src_ref=near.at[source], dst_ref=near.at[source],
-            send_sem=near_send.at[target], recv_sem=near_recv.at[target],
-            device_id=along_y(target), device_id_type=MESH,
-        )
-
-    def part_copy(j, arriving):
+    def near_copy(source, j, heads):
+        return pltpu.make_async_remote_copy(
+            src_ref=near.at[source, heads], dst_ref=near.at[source, heads],
+            send_sem=near_send.at[j], recv_sem=near_recv.at[j, heads],
+            device_id={"sp_1": ring_index(y, j, ny), "tp": mixer_at}, device_id_type=MESH,
+        )
+
+    def part_copy(j, share):
         to = ring_index(y, j, ny)
-        source = ring_index(y, -j, ny) if arriving else y
-        return pltpu.make_async_remote_copy(
-            src_ref=pieces.at[to], dst_ref=parts.at[source],
-            send_sem=part_send.at[j], recv_sem=part_recv.at[j],
-            device_id=along_y(j), device_id_type=MESH,
-        )
-
+        return pltpu.make_async_remote_copy(
+            src_ref=pieces.at[to], dst_ref=parts.at[share, y],
+            send_sem=part_send.at[j], recv_sem=part_recv.at[j, share],
+            device_id={"sp_1": to, "tp": ring_at}, device_id_type=MESH,
+        )
+
+    def part_arrival(j, share):
+        source = ring_index(y, -j, ny)
+        return pltpu.make_async_remote_copy(
+            src_ref=pieces.at[source], dst_ref=parts.at[share, source],
+            send_sem=part_send.at[j], recv_sem=part_recv.at[j, share],
+            device_id={"sp_1": source, "tp": ring_at}, device_id_type=MESH,
+        )
+
+    share = 1 - head_set
     for j in range(1, ny):
-        part_copy(j, False).start()
-    parts[y] = pieces[y]
+        part_copy(j, share).start()
+
+    @pl.when(mixes)
+    def _():
+        part_copy(0, 1).start()
+
+    @pl.when(forwards)
+    def _():
+        parts[0, y] = pieces[y]
+
+    twin_copy = pltpu.make_async_remote_copy(
+        src_ref=exit_ref, dst_ref=exit_both, send_sem=twin_send.at[0], recv_sem=twin_recv.at[0],
+        device_id={"tp": mate}, device_id_type=MESH,
+    )
+
+    @pl.when(forwards)
+    def _():
+        twin_copy.start()
 
     mapping, state, probe, local_out = mixer_end(*begun)
-    near[y] = packed(mapping, state)
+    near[y, head_set] = packed(mapping, state)
     for j in range(1, ny):
-        near_copy(y, j).start()
-    probe_ref[...] = probe
-    local_ref[...] = local_out
-
-    for j in range(1, ny):
-        part_copy(j, True).wait_recv()
-    square = jnp.where(iota((units, wide), 0) == iota((units, wide), 1), 1.0, 0.0).astype(bf16)
-    for c in range(3):
-        tallest = jnp.concatenate(
-            [parts[part, c * rows : (c + 1) * rows, :] for part in range(ny)], axis=0
-        )
-        block = plain(square, tallest, NT).astype(bf16)
-        full_ref[c, :, pl.ds(pl.multiple_of(z * ny * rows, ny * rows), ny * rows)] = block
-
-    def piece(c, at):
-        return full_ref.at[c, :, pl.ds(pl.multiple_of(at * ny * rows, ny * rows), ny * rows)]
-
-    def plus_copy(c, s, at):
-        return pltpu.make_async_remote_copy(
-            src_ref=piece(c, at), dst_ref=piece(c, at),
-            send_sem=plus_send.at[c, s], recv_sem=plus_recv.at[c, s],
+        near_copy(y, j, head_set).start()
+
+    @pl.when(forwards)
+    def _():
+        near_copy(y, 0, 1).start()
+
+    ones = jnp.where(head_blocks(n), 1.0, 0.0)
+    value, switch = v_ref[...].astype(f32), switch_ref[...].astype(f32)
+    bonus = right_exact(r_ref[...].astype(f32) * k_ref[...].astype(f32) * bonus_ref[...], ones)
+    finish_ref[head_set, 0] = probe
+    finish_ref[head_set, 1] = local_out
+    finish_ref[head_set, 2] = rescale_ref[...] * switch
+    finish_ref[head_set, 3] = bonus * value * switch
+    finish_copy = pltpu.make_async_remote_copy(
+        src_ref=finish_ref.at[1], dst_ref=finish_ref.at[1],
+        send_sem=finish_send.at[0], recv_sem=finish_recv.at[0],
+        device_id={"tp": mate}, device_id_type=MESH,
+    )
+
+    @pl.when(forwards)
+    def _():
+        finish_copy.start()
+
+    depth = ny * rows
+
+    def piece(share, at):
+        return full_ref.at[share, :, :, pl.ds(pl.multiple_of(at * depth, depth), depth)]
+
+    def plus_copy(share, s, at):
+        ref = piece(share, at)
+        return pltpu.make_async_remote_copy(
+            src_ref=ref, dst_ref=ref,
+            send_sem=plus_send.at[share, s], recv_sem=plus_recv.at[share, s],
             device_id=along_z(ring_index(z, 1, nz)), device_id_type=MESH,
         )
 
-    def minus_copy(c, s, at):
-        return pltpu.make_async_remote_copy(
-            src_ref=piece(c, at), dst_ref=piece(c, at),
-            send_sem=minus_send.at[c, s], recv_sem=minus_recv.at[c, s],
+    def minus_copy(share, s, at):
+        ref = piece(share, at)
+        return pltpu.make_async_remote_copy(
+            src_ref=ref, dst_ref=ref,
+            send_sem=minus_send.at[share, s], recv_sem=minus_recv.at[share, s],
             device_id=along_z(ring_index(z, -1, nz)), device_id_type=MESH,
         )
 
-    n_plus = nz // 2
+    def hand_copy(at, j):
+        return pltpu.make_async_remote_copy(
+            src_ref=piece(1, at), dst_ref=piece(0, at),
+            send_sem=hand_send.at[j], recv_sem=hand_recv.at[j],
+            device_id={"tp": mate}, device_id_type=MESH,
+        )
+
+    n_plus = max(1, nz // 2 - LESS) if nz > 2 else 1
     n_minus = nz - 1 - n_plus
+    steps = max(n_plus, n_minus) + 1
 
     def ring_step(s):
-        for c in range(3):
+        for share in range(2):
+            after, ahead = ring_index(z, -s, nz), ring_index(z, s, nz)
             if s > 0 and s <= n_plus:
-                plus_copy(c, s - 1, ring_index(z, -s, nz)).wait_recv()
+                plus_copy(share, s - 1, after).wait_recv()
             if s < n_plus:
-                plus_copy(c, s, ring_index(z, -s, nz)).start()
+                plus_copy(share, s, after).start()
             if s > 0 and s <= n_minus:
-                minus_copy(c, s - 1, ring_index(z, s, nz)).wait_recv()
+                minus_copy(share, s - 1, ahead).wait_recv()
             if s < n_minus:
-                minus_copy(c, s, ring_index(z, s, nz)).start()
-
-    ring_step(0)
-    pending = list(range(1, n_plus + 1))
-
-    def ring_steps(count):
-        for s in pending[:count]:
+                minus_copy(share, s, ahead).start()
+            if share == 1:
+                if s <= n_plus:
+                    hand_copy(after, (nz - s) % nz).start()
+                if s > 0 and s <= n_minus:
+                    hand_copy(ahead, s).start()
+
+    @pl.when(forwards)
+    def _():
+        for j in range(1, ny):
+            for share in range(2):
+                part_arrival(j, share).wait_recv()
+        part_copy(0, 1).wait_recv()
+        square = jnp.where(iota((units, wide), 0) == iota((units, wide), 1), 1.0, 0.0).astype(bf16)
+        for share in range(2):
+            for c in range(3):
+                tallest = jnp.concatenate(
+                    [parts[share, part, c * rows : (c + 1) * rows, :] for part in range(ny)], axis=0
+                )
+                block = plain(square, tallest, NT).astype(bf16)
+                full_ref[share, c, :, pl.ds(pl.multiple_of(z * depth, depth), depth)] = block
+        for s in range(max(0, steps - LATER)):
             ring_step(s)
-        del pending[:count]
-
-    for j in range(1, ny):
-        near_copy(ring_index(y, -j, ny), j).wait_recv()
-    before, total = folded(near, ny, y)
-    before_ref[0] = before[0]
-    before_ref[1] = before[1]
+
+    def later_ring_steps(first, end):
+        todo = list(range(max(0, steps - LATER), steps))[first:end]
+        if todo:
+            @pl.when(forwards)
+            def _():
+                for s in todo:
+                    ring_step(s)
 
     def mid_copy(source, j):
         to = z - inner + ring_index(inner, j, span)
@@ -338,78 +412,111 @@
             device_id=along_z(to), device_id_type=MESH,
         )
 
-    mid[inner] = packed(*total)
-    for j in range(1, span):
-        mid_copy(inner, j).start()
-
-    ring_steps(FIRST)
-    for j in range(1, span):
-        mid_copy(ring_index(inner, -j, span), j).wait_recv()
-    before_z, total_z = folded(mid, span, inner)
-    before_ref[2] = before_z[0]
-    before_ref[3] = before_z[1]
-
-    def far_copy(slot, d, to):
-        return pltpu.make_async_remote_copy(
-            src_ref=far.at[slot], dst_ref=far.at[slot],
-            send_sem=far_send.at[d], recv_sem=far_recv.at[d],
+    def far_copy(source, d, to, states_only):
+        ref = far.at[source, 1] if states_only else far.at[source]
+        return pltpu.make_async_remote_copy(
+            src_ref=ref, dst_ref=ref, send_sem=far_send.at[d], recv_sem=far_recv.at[d],
             device_id=along_z(to), device_id_type=MESH,
         )
 
-    far[outer] = packed(*total_z)
-    if nz > 2 * span:
-        pl.semaphore_wait(token_sem, 1)
-    for d in range(1, groups):
-        @pl.when(outer + d < groups)
-        def _():
-            far_copy(outer, d, lax.rem(z + d * span, nz)).start()
-
-    ring_steps(SECOND)
-
-    carry_ref[...] = jnp.zeros((n, n), f32)
-    for g in range(groups - 1):
-        @pl.when(outer > g)
-        def _():
-            for d in range(1, groups):
-                @pl.when(outer - g == d)
-                def _():
-                    far_copy(g, d, lax.rem(z + d * span, nz)).wait_recv()
-            step = unpacked(far[g])
-            carry_ref[...] = left_exact(step[0], carry_ref[...]) + step[1]
-    incoming = fine(before_ref[2], carry_ref[...]) + before_ref[3]
-    incoming = fine(before_ref[0], incoming) + before_ref[1]
-
-    closing = local_ref[...] + fine(probe_ref[...], incoming)
-    ones = jnp.where(head_blocks(n), 1.0, 0.0)
-    centred = closing - right_exact(closing, ones) * (1.0 / WIDTH)
-    spread = right_exact(centred * centred, ones) * (1.0 / WIDTH)
-    rescaled = centred * lax.rsqrt(spread + group_eps) * rescale_ref[...]
-    value = v_ref[...].astype(f32)
-    bonus = right_exact(r_ref[...].astype(f32) * k_ref[...].astype(f32) * bonus_ref[...], ones)
-    bonus = bonus * value
-    mixed = ((rescaled + bonus) * switch_ref[...].astype(f32)).astype(bf16)
+    def far_sends(action):
+        for d in range(1, groups):
+            to = lax.rem(z + d * span, nz)
+
+            @pl.when(outer == 0)
+            def _():
+                getattr(far_copy(0, d, to, True), action)()
+
+            @pl.when((outer > 0) & (outer + d < groups))
+            def _():
+                getattr(far_copy(outer, d, to, False), action)()
+
+    def exit_copy(j, to_core):
+        to = 2 * ring_index(x, j, nx) + to_core
+        return pltpu.make_async_remote_copy(
+            src_ref=sent.at[to], dst_ref=landed.at[j],
+            send_sem=exit_send.at[j, to_core], recv_sem=exit_recv.at[j],
+            device_id={"tp": to}, device_id_type=MESH,
+        )
 
     own = n // nt
     width = exit_ref.shape[1]
 
-    def exit_copy(j):
-        to = ring_index(t, j, nt)
-        return pltpu.make_async_remote_copy(
-            src_ref=sent.at[to], dst_ref=landed.at[j],
-            send_sem=exit_send.at[j], recv_sem=exit_recv.at[j],
-            device_id={"tp": to}, device_id_type=MESH,
-        )
-
-    sent[...] = plain(mixed, exit_ref[...]).astype(bf16).reshape(nt, own, width)
-    for j in range(1, nt):
-        exit_copy(j).start()
-    ring_steps(MIDDLE)
-    attended = sent[t].astype(f32)
-    for j in range(1, nt):
-        exit_copy(j).wait_recv()
-    for j in range(1, nt):
-        attended = attended + landed[j].astype(f32)
-    stream = skip_ref[...].astype(f32) + attended
+    @pl.when(mixes)
+    def _():
+        for j in range(1, ny):
+            for heads in range(2):
+                near_copy(ring_index(y, -j, ny), j, heads).wait_recv()
+        near_copy(y, 0, 1).wait_recv()
+        totals = []
+        for heads in range(2):
+            before, total = folded(near, heads, ny, y)
+            before_ref[heads, 0], before_ref[heads, 1] = before
+            totals.append(packed(*total))
+        for heads in range(2):
+            mid[inner, heads] = totals[heads]
+        for j in range(1, span):
+            mid_copy(inner, j).start()
+        for j in range(1, span):
+            mid_copy(ring_index(inner, -j, span), j).wait_recv()
+        totals = []
+        for heads in range(2):
+            before, total = folded(mid, heads, span, inner)
+            before_ref[heads, 2], before_ref[heads, 3] = before
+            totals.append(packed(*total))
+        far[outer, 0] = jnp.concatenate([part[:WIDTH] for part in totals], axis=0)
+        far[outer, 1] = jnp.concatenate([part[WIDTH:] for part in totals], axis=0)
+        if nz > 2 * span:
+            pl.semaphore_wait(token_sem, 1)
+        far_sends("start")
+        carry_ref[...] = jnp.zeros((2, n, n), f32)
+        finish_copy.wait_recv()
+        twin_copy.wait_recv()
+        for g in range(groups - 1):
+            @pl.when(outer > g)
+            def _():
+                for d in range(1, groups):
+                    @pl.when(outer - g == d)
+                    def _():
+                        far_copy(g, d, lax.rem(z + d * span, nz), g == 0).wait_recv()
+                for heads in range(2):
+                    half = slice(heads * WIDTH, (heads + 1) * WIDTH)
+                    state = unpacked_half(far[g, 1, half])
+                    if g > 0:
+                        state = state + left_exact(unpacked_half(far[g, 0, half]), carry_ref[heads])
+                    carry_ref[heads] = state
+        mixed = []
+        for heads in range(2):
+            incoming = fine(before_ref[heads, 2], carry_ref[heads]) + before_ref[heads, 3]
+            incoming = fine(before_ref[heads, 0], incoming) + before_ref[heads, 1]
+            closing = finish_ref[heads, 1] + fine(finish_ref[heads, 0], incoming)
+            centred = closing - right_exact(closing, ones) * (1.0 / WIDTH)
+            spread = right_exact(centred * centred, ones) * (1.0 / WIDTH)
+            rescaled = centred * lax.rsqrt(spread + group_eps) * finish_ref[heads, 2]
+            mixed.append((rescaled + finish_ref[heads, 3]).astype(bf16))
+        product = plain(
+            jnp.concatenate(mixed, axis=1), jnp.concatenate([exit_ref[...], exit_both[...]], axis=0)
+        )
+        sent[...] = product.astype(bf16).reshape(nt, own, width)
+        for j in range(1, nx):
+            for to_core in range(2):
+                exit_copy(j, to_core).start()
+        exit_copy(0, 1 - MIX).start()
+
+    stream = skip_ref[...].astype(f32)
+    for j in range(1, nx):
+        exit_copy(j, core).wait_recv()
+
+    @pl.when(mixes)
+    def _():
+        landed[0] = sent[t]
+
+    @pl.when(forwards)
+    def _():
+        exit_copy(0, 1 - MIX).wait_recv()
+
+    for j in range(nx):
+        stream = stream + landed[j].astype(f32)
     stream_ref[...] = stream
     mean = jnp.mean(stream * stream, axis=-1, keepdims=True)
     rows_ref[y, x, core] = (stream * lax.rsqrt(mean + norm_eps) * scaling_ref[...]).astype(bf16)
@@ -443,7 +550,7 @@
             device_id=device(ring_index(a, j, na), b), device_id_type=MESH,
         )
 
-    partner = {"tp": t + 1 - 2 * core}
+    partner = {"tp": mate}
 
     def pair_copy(j, i, arriving):
         if arriving:
@@ -461,13 +568,13 @@
     for j in range(1, na):
         two_copy(j, 0, False).start()
     pair_copy(0, 0, False).start()
-    ring_steps(LATE)
+    later_ring_steps(0, 1)
     for i in range(1, na):
         one_copy(i, True).wait_recv()
         for j in range(1, na):
             two_copy(j, i, False).start()
         pair_copy(0, i, False).start()
-    ring_steps(len(pending))
+    later_ring_steps(1, LATER)
     units_at = iota((taps_ref.shape[1], units), 0) == iota((taps_ref.shape[1], units), 1) + y * units
     taps = exact(taps_ref[...], jnp.where(units_at, 1.0, 0.0))
     for i in range(na):
@@ -479,8 +586,13 @@
 
     def projections(c):
         rows = rows_ref[:, :, c].reshape(half, width)
-        gate_rows_ref[:, :, c] = plain(rows, full_ref[0], NT).reshape(ny, nx, own, units)
-        up_rows_ref[:, :, c] = plain(rows, full_ref[1], NT).reshape(ny, nx, own, units)
+        gate_rows_ref[:, :, c] = plain(rows, full_ref[0, 0], NT).reshape(ny, nx, own, units)
+        up_rows_ref[:, :, c] = plain(rows, full_ref[0, 1], NT).reshape(ny, nx, own, units)
+
+    @pl.when(mixes)
+    def _():
+        for j in range(nz):
+            hand_copy(ring_index(z, j, nz), j).wait_recv()
 
     projections(core)
     for i in range(na):
@@ -545,7 +657,7 @@
         )
 
     for p in range(bands):
-        product = plain(hidden, full_ref[2, :, p * band : (p + 1) * band]).astype(bf16)
+        product = plain(hidden, full_ref[0, 2, :, p * band : (p + 1) * band]).astype(bf16)
         partial[p] = product.reshape(ny, nx, 2, own, band)
         swap_copy(p).start()
     order = list(range(1, na)) + [0]
@@ -581,21 +693,35 @@
         out_ref[:, columns] = (stream_ref[:, columns] + projected).astype(bf16)
 
     for j in range(1, ny):
-        near_copy(y, j).wait_send()
-        part_copy(j, False).wait_send()
-    for j in range(1, span):
-        mid_copy(inner, j).wait_send()
-    for d in range(1, groups):
-        @pl.when(outer + d < groups)
-        def _():
-            far_copy(outer, d, lax.rem(z + d * span, nz)).wait_send()
-    for c in range(3):
-        for s in range(n_plus):
-            plus_copy(c, s, ring_index(z, -s, nz)).wait_send()
-        for s in range(n_minus):
-            minus_copy(c, s, ring_index(z, s, nz)).wait_send()
-    for j in range(1, nt):
-        exit_copy(j).wait_send()
+        near_copy(y, j, head_set).wait_send()
+        part_copy(j, 1 - head_set).wait_send()
+
+    @pl.when(mixes)
+    def _():
+        part_copy(0, 1).wait_send()
+        for j in range(1, span):
+            mid_copy(inner, j).wait_send()
+        far_sends("wait_send")
+        for j in range(1, nx):
+            for to_core in range(2):
+                exit_copy(j, to_core).wait_send()
+        exit_copy(0, 1 - MIX).wait_send()
+
+    @pl.when(forwards)
+    def _():
+        if nz > 2 * span:
+            pl.semaphore_wait(token_sem, 1)
+        near_copy(y, 0, 1).wait_send()
+        twin_copy.wait_send()
+        finish_copy.wait_send()
+        for share in range(2):
+            for s in range(n_plus):
+                plus_copy(share, s, ring_index(z, -s, nz)).wait_send()
+            for s in range(n_minus):
+                minus_copy(share, s, ring_index(z, s, nz)).wait_send()
+        for j in range(nz):
+            hand_copy(ring_index(z, j, nz), j).wait_send()
+
     for j in range(1, na):
         one_copy(j, False).wait_send()
         for p in range(bands):
@@ -628,7 +754,6 @@
     band = width // BANDS
     dma = pltpu.SemaphoreType.DMA
     in_vmem = pl.BlockSpec(memory_space=pltpu.VMEM)
-    n_plus = nz // 2
     edge = 16
     return pl.pallas_call(
         functools.partial(layer_kernel, nz, ny, nt, span, len(args)),
@@ -638,18 +763,18 @@
         scratch_shapes=[pltpu.VMEM(arg.shape, arg.dtype) for arg in args]
         + [
             dma((len(args),)),
-            pltpu.VMEM((3, units, nz * ny * rows), bf16),
-            pltpu.VMEM((ny, n, n), bf16),
-            pltpu.VMEM((span, n, n), bf16),
-            pltpu.VMEM((groups, n, n), bf16),
+            pltpu.VMEM((2, 3, units, nz * ny * rows), bf16),
+            pltpu.VMEM((ny, 2, n, n), bf16),
+            pltpu.VMEM((span, 2, n, n), bf16),
+            pltpu.VMEM((groups, 2, n, n), bf16),
             pltpu.VMEM((ny, 3 * rows, wide), bf16),
-            pltpu.VMEM((ny, 3 * rows, wide), bf16),
-            pltpu.VMEM((n, n), f32),
-            pltpu.VMEM((n, n), f32),
-            pltpu.VMEM((4, n, n), f32),
-            pltpu.VMEM((n, n), f32),
+            pltpu.VMEM((2, ny, 3 * rows, wide), bf16),
+            pltpu.VMEM((2, 4, n, n), f32),
+            pltpu.VMEM((2, 4, n, n), f32),
+            pltpu.VMEM((2, n, n), f32),
+            pltpu.VMEM((n, width), bf16),
             pltpu.VMEM((nt, own, width), bf16),
-            pltpu.VMEM((nt, own, width), bf16),
+            pltpu.VMEM((nx, own, width), bf16),
             pltpu.VMEM((own, width), f32),
             pltpu.VMEM((ny, nx, 2, own, width), bf16),
             pltpu.VMEM((edge + ny * n, units), f32),
@@ -664,10 +789,11 @@
             pltpu.VMEM((ny, nx, 2, own, units), f32),
             pltpu.VMEM((ny, nx, 2, own, units), f32),
             pltpu.SemaphoreType.REGULAR,
-            dma((ny,)), dma((ny,)), dma((span,)), dma((span,)), dma((groups,)), dma((groups,)),
-            dma((ny,)), dma((ny,)),
-            dma((3, n_plus)), dma((3, n_plus)), dma((3, n_plus)), dma((3, n_plus)),
-            dma((nt,)), dma((nt,)), dma((nx,)), dma((nx,)),
+            dma((ny,)), dma((ny, 2)), dma((span,)), dma((span,)), dma((groups,)), dma((groups,)),
+            dma((ny,)), dma((ny, 2)),
+            dma((2, nz)), dma((2, nz)), dma((2, nz)), dma((2, nz)),
+            dma((1,)), dma((1,)), dma((1,)), dma((1,)), dma((nz,)), dma((nz,)),
+            dma((nx, 2)), dma((nx,)), dma((nx,)), dma((nx,)),
             dma((ny, nx)), dma((ny, nx)), dma((ny, nx)), dma((ny, nx)),
             dma((1,)), dma((1,)), dma((BANDS,)), dma((BANDS,)),
             dma((BANDS, ny)), dma((BANDS, ny)), dma((BANDS, nx)), dma((BANDS, nx)),

time: 84 us -> 79.4 us (0.945)
  the two profiles are of different devices: /device:TPU:32 before, /device:TPU:36 now
where the time goes in v4:
time: 79.4 us; the launch traced here: 79.2 us
  Pallas kernels  77.7 us (98%)
  local copies, waits for them, and re-layouts  1.47 us (2%)
    pallas_call x1, Pallas kernels, layer(): pl.pallas_call(functools.partial(layer_kernel, nz, ny, nt, span, len(args...  77.7 us

profile of v4, /device:TPU:36, one launch (start us, length us, event | category | flops | bytes accessed | tf_op | source)
XLA Modules:
  0.0 79.2 jit_solution(13730309989591153828)
XLA Ops:
  0.0 77.7 %layer.1 = bf16[16,2048]{1,0:T(8,128)(2,1)} custom-call(bf16[128,128]{1,0:T(8,128)(2,1)} %refs_0_.1, bf16[128,128]{1,0:T(8,128)(2,1)} %refs_1_.1, bf16[128,128]{1,0:T(8,128)(2,1)} %refs_2_.1, f32[128,128]{1,0:T(8,128)} %refs_3_.1, f32[128,128]{1,0:T(8,128)} %refs_4_.1, bf16[128,128]{1,0:T(8,128)(2,1)} %refs_5_.1, f32[1,128]{1,0:T(1,128)} %bitcast.6, ...), custom_call_target="tpu_custom_call" | custom-call | tf_op jit(solution)/shard_map/layer/pallas_call | solution.py:758
  77.7 1.5 %copy.17 = bf16[16,2048]{1,0:T(8,128)(2,1)} copy(bf16[16,2048]{1,0:T(8,128)(2,1)} %layer.1) | data formatting | bytes 131072

commit v5 on v4

--- a/solution.py
+++ b/solution.py
@@ -14,7 +14,7 @@
 COLUMNS = 4
 BANDS = 4
 SPLIT = 16
-MIX, LATER, LESS = 0, 2, 1
+MIX, LATER, LESS = 0, 3, 1
 MESH = pl.DeviceIdType.MESH
 
 group_eps = 0.00064
@@ -472,6 +472,13 @@
         carry_ref[...] = jnp.zeros((2, n, n), f32)
         finish_copy.wait_recv()
         twin_copy.wait_recv()
+        for heads in range(2):
+            map_y, state_y, map_z, state_z = (before_ref[heads, k] for k in range(4))
+            shown = fine(map_y, jnp.concatenate([map_z, state_z], axis=1))
+            entry = jnp.concatenate([shown[:, :n], shown[:, n:] + state_y], axis=1)
+            seen = fine(finish_ref[heads, 0], entry)
+            finish_ref[heads, 0] = seen[:, :n]
+            finish_ref[heads, 1] = finish_ref[heads, 1] + seen[:, n:]
         for g in range(groups - 1):
             @pl.when(outer > g)
             def _():
@@ -487,9 +494,7 @@
                     carry_ref[heads] = state
         mixed = []
         for heads in range(2):
-            incoming = fine(before_ref[heads, 2], carry_ref[heads]) + before_ref[heads, 3]
-            incoming = fine(before_ref[heads, 0], incoming) + before_ref[heads, 1]
-            closing = finish_ref[heads, 1] + fine(finish_ref[heads, 0], incoming)
+            closing = finish_ref[heads, 1] + fine(finish_ref[heads, 0], carry_ref[heads])
             centred = closing - right_exact(closing, ones) * (1.0 / WIDTH)
             spread = right_exact(centred * centred, ones) * (1.0 / WIDTH)
             rescaled = centred * lax.rsqrt(spread + group_eps) * finish_ref[heads, 2]
@@ -568,6 +573,8 @@
     for j in range(1, na):
         two_copy(j, 0, False).start()
     pair_copy(0, 0, False).start()
+    units_at = iota((taps_ref.shape[1], units), 0) == iota((taps_ref.shape[1], units), 1) + y * units
+    taps = exact(taps_ref[...], jnp.where(units_at, 1.0, 0.0))
     later_ring_steps(0, 1)
     for i in range(1, na):
         one_copy(i, True).wait_recv()
@@ -575,8 +582,6 @@
             two_copy(j, i, False).start()
         pair_copy(0, i, False).start()
     later_ring_steps(1, LATER)
-    units_at = iota((taps_ref.shape[1], units), 0) == iota((taps_ref.shape[1], units), 1) + y * units
-    taps = exact(taps_ref[...], jnp.where(units_at, 1.0, 0.0))
     for i in range(na):
         for j in range(1, na):
             two_copy(j, i, True).wait_recv()

time: 79.4 us -> 78.5 us (0.989)
  the two profiles are of different devices: /device:TPU:36 before, /device:TPU:480 now
where the time goes in v5:
time: 78.5 us; the launch traced here: 78.3 us
  Pallas kernels  76.8 us (98%)
  local copies, waits for them, and re-layouts  1.47 us (2%)
    pallas_call x1, Pallas kernels, layer(): pl.pallas_call(functools.partial(layer_kernel, nz, ny, nt, span, len(args...  76.8 us

profile of v5, /device:TPU:480, one launch (start us, length us, event | category | flops | bytes accessed | tf_op | source)
XLA Modules:
  0.0 78.3 jit_solution(16072020869227548650)
XLA Ops:
  0.0 76.8 %layer.1 = bf16[16,2048]{1,0:T(8,128)(2,1)} custom-call(bf16[128,128]{1,0:T(8,128)(2,1)} %refs_0_.1, bf16[128,128]{1,0:T(8,128)(2,1)} %refs_1_.1, bf16[128,128]{1,0:T(8,128)(2,1)} %refs_2_.1, f32[128,128]{1,0:T(8,128)} %refs_3_.1, f32[128,128]{1,0:T(8,128)} %refs_4_.1, bf16[128,128]{1,0:T(8,128)(2,1)} %refs_5_.1, f32[1,128]{1,0:T(1,128)} %bitcast.6, ...), custom_call_target="tpu_custom_call" | custom-call | tf_op jit(solution)/shard_map/layer/pallas_call | solution.py:763
  76.8 1.5 %copy.17 = bf16[16,2048]{1,0:T(8,128)(2,1)} copy(bf16[16,2048]{1,0:T(8,128)(2,1)} %layer.1) | data formatting | bytes 131072
